TPU v7x, 32 devices: a whole 2x2x4 slice. The times are simulated.
32 devices in a mesh: sp: 8 (over z, x), tp: 4 (over y, core).
Axes of the slice: x: 2, y: 2, z: 4, core: 2. Of those that a mesh axis runs over, the one named last changes fastest.
Arguments:
- tokens: bfloat16 [6144, 4096], P('sp', 'tp'), may hold values from -12 to 12
- query_weight: bfloat16 [4096, 2048], P(None, 'tp'), may hold values from -0.09375 to 0.09375
- key_weight: bfloat16 [4096, 2048], P(None, 'tp'), may hold values from -0.09375 to 0.09375
- value_weight: bfloat16 [4096, 2048], P(None, 'tp'), may hold values from -0.09375 to 0.09375
- position_bias: float32 [16, 320], P('tp'), may hold values from -104 to 154
- out_grad: bfloat16 [6144, 2048], P('sp', 'tp'), may hold values from -6 to 6
Outputs:
- input_grad: bfloat16 [6144, 4096], P('sp', 'tp')
- query_weight_grad: float32 [4096, 2048], P('sp', 'tp')
- key_weight_grad: float32 [4096, 2048], P('sp', 'tp')
- value_weight_grad: float32 [4096, 2048], P('sp', 'tp')
- bias_grad: float32 [16, 320], P('tp')
All inputs are finite; a program needn't handle non-finite values.
Results may differ from a plain program's by a relative error of at most 0.014.
Values may be sent and summed in bfloat16 or wider, within the bound.
A program may use at most 128 MiB of HBM per device.

v0:
```python
import jax
import jax.numpy as jnp
import numpy as np
from jax import lax
from jax.sharding import PartitionSpec as P

SEGMENT = 64
PREVIOUS = 4
CLIP = 256


def from_behind(value, axis, steps):
    count = lax.axis_size(axis)
    leading, last = (max(0, -steps), min(count, count - steps))
    return lax.ppermute(value, axis, [(source, source + steps) for source in range(leading, last)])


def band_view(extended, count, heads, head):
    shaped = extended.reshape(count + PREVIOUS, SEGMENT, heads, head)
    stacked = jnp.stack([shaped[band : band + count] for band in range(PREVIOUS + 1)], axis=1)
    return stacked.reshape(count, (PREVIOUS + 1) * SEGMENT, heads, head)


def fold_band(parts, count):
    heads = parts.shape[2]
    head = parts.shape[3]
    shaped = parts.reshape(count, PREVIOUS + 1, SEGMENT, heads, head)
    total = jnp.zeros((count + PREVIOUS, SEGMENT, heads, head), jnp.float32)
    for band in range(PREVIOUS + 1):
        total = total + jnp.pad(shaped[:, band], ((band, PREVIOUS - band), (0, 0), (0, 0), (0, 0)))
    return total.reshape((count + PREVIOUS) * SEGMENT, heads * head)


def diagonal_table(reach, table_len):
    diagonals = reach + 2 * SEGMENT - 1
    distance = reach + SEGMENT - 1 - np.arange(diagonals)
    target = np.minimum(distance, CLIP) + SEGMENT - 1
    return (
        target.astype(np.int32),
        (target[:, None] == np.arange(table_len)[None, :]).astype(np.float32),
    )


def contract_rows(left, right):
    return lax.dot_general(
        left, right, (((0,), (0,)), ((), ())), preferred_element_type=jnp.float32
    )


def contract_cols(left, right):
    return lax.dot_general(
        left, right, (((1,), (1,)), ((), ())), preferred_element_type=jnp.float32
    )


def shards(tokens, query_weight, key_weight, value_weight, position_bias, out_grad):
    whole = lax.all_gather(tokens, "tp", axis=1, tiled=True)
    query = jnp.dot(whole, query_weight, preferred_element_type=jnp.float32).astype(jnp.bfloat16)
    keys = jnp.dot(whole, key_weight, preferred_element_type=jnp.float32).astype(jnp.bfloat16)
    values = jnp.dot(whole, value_weight, preferred_element_type=jnp.float32).astype(jnp.bfloat16)
    length, width = query.shape
    heads = position_bias.shape[0]
    head = width // heads
    reach = PREVIOUS * SEGMENT
    span = reach + SEGMENT
    count = length // SEGMENT
    factor = head ** (-0.5)
    prev_keys, prev_values = from_behind(
        (keys[length - reach :], values[length - reach :]), "sp", 1
    )
    key_band = band_view(jnp.concatenate([prev_keys, keys]), count, heads, head)
    value_band = band_view(jnp.concatenate([prev_values, values]), count, heads, head)
    query_seg = query.reshape(count, SEGMENT, heads, head)
    grad_seg = out_grad.reshape(count, SEGMENT, heads, head)
    target, fold_map = diagonal_table(reach, position_bias.shape[1])
    along = position_bias[:, target]
    bias = jnp.stack(
        [along[:, SEGMENT - 1 - row : SEGMENT - 1 - row + span] for row in range(SEGMENT)], axis=1
    )
    scores = (
        jnp.einsum("cqhd,ckhd->hcqk", query_seg, key_band, preferred_element_type=jnp.float32)
        * factor
        + bias[:, None]
    )
    offset = lax.axis_index("sp") * length
    key_pos = offset - reach + jnp.arange(count)[:, None] * SEGMENT + jnp.arange(span)[None, :]
    valid = (key_pos >= 0)[None, :, None, :]
    masked = jnp.where(valid, scores, -jnp.inf)
    top = jnp.max(masked, axis=-1, keepdims=True)
    logsum = top + jnp.log(jnp.sum(jnp.exp(masked - top), axis=-1, keepdims=True))
    weights = jnp.exp(masked - logsum)
    weights_low = weights.astype(jnp.bfloat16)
    prob_grad = jnp.einsum(
        "cqhd,ckhd->hcqk", grad_seg, value_band, preferred_element_type=jnp.float32
    )
    delta = jnp.sum(weights * prob_grad, axis=-1, keepdims=True)
    score_grad = weights * (prob_grad - delta)
    score_low = score_grad.astype(jnp.bfloat16)
    query_grad = (
        (
            jnp.einsum("hcqk,ckhd->cqhd", score_low, key_band, preferred_element_type=jnp.float32)
            * factor
        )
        .reshape(length, width)
        .astype(jnp.bfloat16)
    )
    key_parts = (
        jnp.einsum("hcqk,cqhd->ckhd", score_low, query_seg, preferred_element_type=jnp.float32)
        * factor
    )
    value_parts = jnp.einsum(
        "hcqk,cqhd->ckhd", weights_low, grad_seg, preferred_element_type=jnp.float32
    )
    key_total = fold_band(key_parts, count)
    value_total = fold_band(value_parts, count)
    back_keys, back_values = from_behind((key_total[:reach], value_total[:reach]), "sp", -1)
    edge_pad = ((length - reach, 0), (0, 0))
    key_grad = (key_total[reach:] + jnp.pad(back_keys, edge_pad)).astype(jnp.bfloat16)
    value_grad = (value_total[reach:] + jnp.pad(back_values, edge_pad)).astype(jnp.bfloat16)
    bias_terms = jnp.sum(score_grad, axis=1)[:, ::-1, :]
    skewed = jnp.pad(bias_terms, ((0, 0), (0, 0), (0, SEGMENT))).reshape(
        heads, SEGMENT * (span + SEGMENT)
    )
    skewed = skewed[:, : SEGMENT * (span + SEGMENT - 1)].reshape(heads, SEGMENT, span + SEGMENT - 1)
    diagonal_sums = jnp.sum(skewed, axis=1)
    bias_local = jnp.dot(
        diagonal_sums,
        jnp.asarray(fold_map),
        precision=lax.Precision.HIGHEST,
        preferred_element_type=jnp.float32,
    )
    bias_grad = lax.psum(bias_local, "sp")
    input_part = (
        contract_cols(query_grad, query_weight)
        + contract_cols(key_grad, key_weight)
        + contract_cols(value_grad, value_weight)
    )
    input_grad = lax.psum_scatter(
        input_part.astype(jnp.bfloat16), "tp", scatter_dimension=1, tiled=True
    )
    stacked = jnp.concatenate([query_grad, key_grad, value_grad], axis=1)
    weight_grad = lax.psum_scatter(
        contract_rows(whole, stacked), "sp", scatter_dimension=0, tiled=True
    )
    return (
        input_grad,
        weight_grad[:, :width],
        weight_grad[:, width : 2 * width],
        weight_grad[:, 2 * width :],
        bias_grad,
    )


def solution(mesh):
    in_specs = (
        P("sp", "tp"),
        P(None, "tp"),
        P(None, "tp"),
        P(None, "tp"),
        P("tp", None),
        P("sp", "tp"),
    )
    out_specs = (P("sp", "tp"), P("sp", "tp"), P("sp", "tp"), P("sp", "tp"), P("tp", None))
    return jax.shard_map(shards, mesh=mesh, in_specs=in_specs, out_specs=out_specs, check_vma=False)
```

profile of v0, /device:TPU:0, one launch (start us, length us, event | category | flops | bytes accessed | tf_op | source)
XLA Modules:
  0.0 686.2 jit_solution(1822297870764970203)
XLA Ops:
  9.5 1.1 gather_fusion
  42.7 15.9 %all-gather.2.cloned.1.call-done = bf16[768,4096]{1,0:T(8,128)(2,1)} async-done(((bf16[768,1024]{1,0:T(8,128)(2,1)}), bf16[768,4096]{1,0:T(8,128)(2,1)}) %all-gather.2.cloned.1.call-update) | async-done | bytes 6291472 | tf_op jit(solution)/shard_map/all_gather | solution.py:57
  58.7 7.5 %convolution_convert_fusion.2 = bf16[768,512]{1,0:T(8,128)(2,1)S(1)} fusion(bf16[768,4096]{1,0:T(8,128)(2,1)} %all-gather.2.cloned.1.call-done, bf16[4096,512]{1,0:T(8,128)(2,1)} %param.11), kind=kOutput, calls=%fused_computation.48 | convolution fusion | flops 3221618688 | bytes 11272192 | tf_op jit(solution)/shard_map/dot_general | solution.py:59
  66.9 4.5 collective-permute-start
  71.4 3.4 convolution_convert_fusion.1
  74.9 3.4 convolution_convert_fusion
  78.3 1.1 stack.235
  80.1 1.1 stack.306
  81.4 3.4 collective-permute-start.1
  84.8 2.6 pad_maximum_fusion.1
  87.4 2.5 stack.231
  89.9 2.4 constant_dynamic-update-slice_fusion.4
  92.3 2.4 stack.232
  94.7 1.1 stack.233
  95.8 1.1 stack.234
  96.8 2.5 constant_dynamic-update-slice_fusion.3
  99.3 1.2 constant_dynamic-update-slice_fusion.2
  100.6 1.2 constant_dynamic-update-slice_fusion.1
  101.8 1.2 constant_dynamic-update-slice_fusion
  103.0 3.2 copy.152
  106.2 1.6 fusion.38
  107.8 1.3 exponential_reduce_fusion
  109.9 2.5 fusion.8
  112.5 1.5 fusion.34
  114.0 1.0 copy.294
  115.0 2.5 copy_bitcast_fusion.2
  117.5 2.5 copy_bitcast_fusion
  120.2 1.9 copy-done.1
  122.1 3.0 copy.241
  125.9 1.3 collective-permute-start.3
  127.2 1.5 pad_add_fusion
  129.8 2.8 pad_maximum_fusion
  132.7 2.5 stack.302
  135.1 2.4 constant_dynamic-update-slice_fusion.9
  137.5 2.4 stack.303
  139.9 2.4 stack.304
  142.4 2.4 stack.305
  144.8 2.5 constant_dynamic-update-slice_fusion.8
  147.3 2.4 constant_dynamic-update-slice_fusion.7
  149.6 1.2 constant_dynamic-update-slice_fusion.6
  150.8 1.2 constant_dynamic-update-slice_fusion.5
  152.0 3.3 copy.219
  155.4 1.5 fusion.29
  156.9 17.5 %fusion.36 = (f32[4,64,320]{2,1,0:T(8,128)S(1)}, bf16[4,12,64,320]{3,2,1,0:T(8,128)(2,1)S(1)}) fusion(f32[4,12,320,64]{2,3,1,0:T(8,128)S(1)} %fusion.29, f32[4,12,64,320]{3,2,1,0:T(8,128)S(1)} %bitcast.228, f32[4,12,64]{2,1,0:T(8,128)S(1)} %copy-done.16), kind=kOutput, calls=%fused_computation.157 | output fusion | flops 6802751 | bytes 10170368 | tf_op jit(solution)/shard_map/sub | solution.py:97
  174.4 1.3 broadcast_multiply_fusion
  175.7 1.5 fusion.35
  178.3 2.5 copy_bitcast_fusion.7
  180.8 2.5 copy_bitcast_fusion.5
  183.3 1.1 pad_add_fusion.1
  184.7 1.6 collective-permute-start.2
  186.2 1.1 copy-done.2
  189.1 1.3 fusion.13
  190.4 10.7 %collective-permute-done.2 = f32[256,512]{1,0:T(8,128)S(1)} collective-permute-done((f32[256,512]{1,0:T(8,128)S(1)}, f32[256,512]{1,0:T(8,128)S(1)}, u32[]{:S(2)}, u32[]{:S(2)}) %collective-permute-start.2) | collective-permute-done | bytes 524320 | tf_op jit(solution)/shard_map/ppermute | solution.py:15
  201.3 13.9 %convolution_bitcast_fusion = f32[4096,1536]{0,1:T(8,128)} fusion(bf16[768,4096]{1,0:T(8,128)(2,1)S(1)} %bitcast.248, bf16[768,512]{1,0:T(8,128)(2,1)S(1)} %fusion.13, bf16[768,512]{1,0:T(8,128)(2,1)S(1)} %fusion.14, bf16[768,512]{1,0:T(8,128)(2,1)S(1)} %bitcast.245), kind=kOutput, calls=%fused_computation.2 | convolution fusion | flops 9670754304 | bytes 33816576 | tf_op jit(solution)/shard_map/dot_general | solution.py:45
  215.3 9.3 %fusion.33 = f32[768,4096]{1,0:T(8,128)} fusion(bf16[4096,512]{1,0:T(8,128)(2,1)} %param.10, bf16[96,8,4,128]{3,2,1,0:T(4,128)(2,1)S(1)} %bitcast.241), kind=kOutput, calls=%fused_computation.154 | convolution fusion | flops 3221225472 | bytes 17563648 | tf_op jit(solution)/shard_map/dot_general | solution.py:51
  224.6 6.4 fusion.39
  231.0 14.1 %add_convert_fusion = bf16[768,4096]{1,0:T(8,128)(2,1)} fusion(f32[768,4096]{1,0:T(8,128)} %fusion.33, f32[768,4096]{1,0:T(8,128)} %fusion.39, bf16[768,512]{1,0:T(8,128)(2,1)S(1)} %fusion.13, bf16[4096,512]{1,0:T(8,128)(2,1)} %param.12), kind=kOutput, calls=%fused_computation.3 | convolution fusion | flops 3230662656 | bytes 36438016 | tf_op jit(solution)/shard_map/dot_general | solution.py:51
  246.6 22.0 %psum.7 = f32[4,320]{1,0:T(4,128)} all-reduce(f32[4,320]{1,0:T(4,128)S(1)} %fusion.40), channel_id=1, replica_groups=mesh['sp'=8,'tp'=4] {'sp'}, use_global_device_ids=true, to_apply=%region_7.8 | all-reduce | flops 1280 | bytes 10240 | tf_op jit(solution)/shard_map/psum | solution.py:132
  268.6 350.7 %reduce-scatter.5.cloned.1.call-done = f32[512,1536]{0,1:T(8,128)} async-done(((f32[4096,1536]{0,1:T(8,128)}), f32[512,1536]{0,1:T(8,128)}) %reduce-scatter.5.cloned.1.call-update) | async-done | bytes 3145744 | tf_op jit(solution)/shard_map/reduce_scatter | solution.py:142
  619.3 2.2 fusion.37
  621.5 1.3 copy.238
  622.8 1.3 copy.239
  624.1 1.3 copy.240
  625.4 54.1 %reduce-scatter.3.cloned.1.call-done = bf16[768,1024]{1,0:T(8,128)(2,1)} async-done(((bf16[768,4096]{1,0:T(8,128)(2,1)}), bf16[768,1024]{1,0:T(8,128)(2,1)}) %reduce-scatter.3.cloned.1.call-update) | async-done | bytes 1572880 | tf_op jit(solution)/shard_map/reduce_scatter | solution.py:138
  (229 shorter events, 43.0 us)
Async XLA Ops:
  7.2 51.5 %all-gather.2.cloned.1.call-start = ((), (), s32[]{:S(2)}) async-start(), calls=%async_computation.2 | async-start | bytes 7864320 | tf_op jit(solution)/shard_map/all_gather | solution.py:57
  7.9 611.4 %reduce-scatter.5.cloned.1.call-start = ((), (), s32[]{:S(2)}) async-start(), calls=%async_computation.4 | async-start | bytes 28311552 | tf_op jit(solution)/shard_map/reduce_scatter | solution.py:142
  39.3 2.1 copy-start.13
  40.1 1.5 copy-start.17
  40.1 1.5 copy-start.18
  40.1 1.5 copy-start.19
  40.1 1.5 copy-start.20
  40.1 1.5 copy-start.21
  40.1 1.5 copy-start.22
  40.1 1.5 copy-start.23
  40.2 1.5 copy-start.24
  40.2 1.5 copy-start.25
  40.2 1.5 copy-start.26
  40.2 1.5 copy-start.27
  40.2 1.5 copy-start.28
  40.2 1.5 copy-start.29
  40.2 1.5 copy-start.30
  40.2 1.5 copy-start.31
  40.2 1.5 copy-start.32
  40.2 1.5 copy-start.33
  40.3 1.5 copy-start.34
  40.3 1.5 copy-start.35
  40.3 1.5 copy-start.36
  40.3 1.5 copy-start.37
  40.3 1.5 copy-start.38
  40.3 1.5 copy-start.39
  40.3 1.5 copy-start.40
  40.3 1.5 copy-start.41
  40.3 1.5 copy-start.42
  40.3 1.5 copy-start.43
  40.4 1.5 copy-start.44
  40.4 1.5 copy-start.45
  40.4 1.5 copy-start.46
  40.4 1.5 copy-start.47
  40.4 1.5 copy-start.48
  40.4 1.5 copy-start.49
  40.4 1.5 copy-start.50
  58.7 12.8 %copy-start.55 = (bf16[768,4096]{1,0:T(8,128)(2,1)S(1)}, bf16[768,4096]{1,0:T(8,128)(2,1)}, u32[]{:S(2)}) copy-start(bf16[768,4096]{1,0:T(8,128)(2,1)} %all-gather.2.cloned.1.call-done) | copy-start | bytes 18874372
  58.7 12.8 %copy-start.56 = (bf16[4096,512]{1,0:T(8,128)(2,1)S(1)}, bf16[4096,512]{1,0:T(8,128)(2,1)}, u32[]{:S(2)}) copy-start(bf16[4096,512]{1,0:T(8,128)(2,1)} %param.10) | copy-start | bytes 12582916
  66.9 7.9 %copy-start.6 = (bf16[4096,512]{1,0:T(8,128)(2,1)S(1)}, bf16[4096,512]{1,0:T(8,128)(2,1)}, u32[]{:S(2)}) copy-start(bf16[4096,512]{1,0:T(8,128)(2,1)} %param.12) | copy-start | bytes 12582916
  66.9 17.9 %collective-permute-start = (bf16[256,512]{1,0:T(8,128)(2,1)}, bf16[256,512]{1,0:T(8,128)(2,1)}, u32[]{:S(2)}, u32[]{:S(2)}) collective-permute-start(bf16[256,512]{1,0:T(8,128)(2,1)} %slice.398), channel_id=1, source_target_pairs={{0,4},{4,8},{8,12},{12,16},{16,20},{20,24},{24,28},{1,5},{5,9},{9,... | collective-permute-start | bytes 786440 | tf_op jit(solution)/shard_map/ppermute | solution.py:15
  78.3 1.9 copy-start.4
  81.4 47.4 %collective-permute-start.1 = (bf16[256,512]{1,0:T(8,128)(2,1)}, bf16[256,512]{1,0:T(8,128)(2,1)}, u32[]{:S(2)}, u32[]{:S(2)}) collective-permute-start(bf16[256,512]{1,0:T(8,128)(2,1)} %slice.469), channel_id=1, source_target_pairs={{0,4},{4,8},{8,12},{12,16},{16,20},{20,24},{24,28},{1,5},{5,9},{9,... | collective-permute-start | bytes 786440 | tf_op jit(solution)/shard_map/ppermute | solution.py:15
  87.4 7.3 %copy-start.7 = (bf16[768,512]{1,0:T(8,128)(2,1)S(1)}, bf16[768,512]{1,0:T(8,128)(2,1)}, u32[]{:S(2)}) copy-start(bf16[768,512]{1,0:T(8,128)(2,1)} %get-tuple-element.47) | copy-start | bytes 2359300
  95.8 3.6 copy-start.10
  96.8 3.7 copy-start.11
  96.8 5.0 copy-start.9
  107.8 2.2 copy-start
  109.9 2.5 copy-start.15
  120.0 2.1 copy-start.1
  125.9 63.2 %collective-permute-start.3 = (f32[256,512]{1,0:T(8,128)}, f32[256,512]{1,0:T(8,128)}, u32[]{:S(2)}, u32[]{:S(2)}) collective-permute-start(f32[256,512]{1,0:T(8,128)} %bitcast.220), channel_id=1, source_target_pairs={{4,0},{8,4},{12,8},{16,12},{20,16},{24,20},{28,24},{5,1},{9,5},{13... | collective-permute-start | bytes 1572872 | tf_op jit(solution)/shard_map/ppermute | solution.py:15
  144.8 4.8 copy-start.12
  144.8 6.0 copy-start.8
  152.0 4.8 slice-start
  155.3 1.5 slice-start.1
  155.4 1.5 copy-start.16
  184.4 1.8 copy-start.3
  184.6 2.7 copy-start.2
  184.6 16.7 %slice-start.3 = ((s8[6291456]{0:T(1024)(128)(4,1)}), s8[4194304]{0:T(1024)(128)(4,1)S(1)}, s32[]{:S(2)}) async-start(s8[6291456]{0:T(1024)(128)(4,1)} %bitcast.247), calls=%async_computation.8 | async-start | bytes 8388608
  184.7 16.4 %collective-permute-start.2 = (f32[256,512]{1,0:T(8,128)S(1)}, f32[256,512]{1,0:T(8,128)S(1)}, u32[]{:S(2)}, u32[]{:S(2)}) collective-permute-start(f32[256,512]{1,0:T(8,128)S(1)} %bitcast.246), channel_id=1, source_target_pairs={{4,0},{8,4},{12,8},{16,12},{20,16},{24,20},{28,24},{5,1},{9,5},{13... | collective-permute-start | bytes 1572872 | tf_op jit(solution)/shard_map/ppermute | solution.py:15
  187.3 14.0 %slice-start.4 = ((s8[6291456]{0:T(1024)(128)(4,1)}), s8[2097152]{0:T(1024)(128)(4,1)S(1)}, s32[]{:S(2)}) async-start(s8[6291456]{0:T(1024)(128)(4,1)} %bitcast.247), calls=%async_computation.9 | async-start | bytes 4194304
  188.9 12.2 %slice-start.2 = ((f32[16,64,4,128]{3,2,1,0:T(4,128)}), f32[12,64,4,128]{3,2,1,0:T(4,128)S(1)}, s32[]{:S(2)}) async-start(f32[16,64,4,128]{3,2,1,0:T(4,128)} %copy-done.3), calls=%async_computation.7 | async-start | bytes 3145728 | tf_op jit(solution)/shard_map/slice | solution.py:118
  215.3 464.2 %reduce-scatter.3.cloned.1.call-start = ((), (), s32[]{:S(2)}) async-start(), calls=%async_computation.3 | async-start | bytes 7864320 | tf_op jit(solution)/shard_map/reduce_scatter | solution.py:138
  215.3 9.3 %copy-start.57 = (bf16[4096,512]{1,0:T(8,128)(2,1)S(1)}, bf16[4096,512]{1,0:T(8,128)(2,1)}, u32[]{:S(2)}) copy-start(bf16[4096,512]{1,0:T(8,128)(2,1)} %param.11) | copy-start | bytes 12582916
  (6 other events, 8.1 us)
Sparse Core Ops, SparseCore 0:
  9.5 49.0 all-gather.1
  215.4 403.9 reduce-scatter.4
  622.5 56.9 reduce-scatter.2
where the time goes:
time: 693 us; the launch traced here: 686 us
  waiting for transfers between devices  432 us (62%)
  local copies, waits for them, and re-layouts  110 us (16%)
  matrix products  66.3 us (10%)
  other arithmetic  29.4 us (4%)
  blocking collectives  22 us (3%)
  between operations  15.2 us (2%)
  starting transfers between devices  10.9 us (2%)
    reduce_scatter x1, waiting for transfers between devices, shards(): lax.psum_scatter(contract_rows(whole, stacked), 'sp', scatter_dimension=0...  351 us
    reduce_scatter x1, waiting for transfers between devices, shards(): lax.psum_scatter(input_part.astype(jnp.bfloat16), 'tp', scatter_dimension...  54.1 us
    another operation x69, local copies, waits for them, and re-layouts, shards(): jnp.stack([along[:, SEGMENT - 1 - row:SEGMENT - 1 - row + span] for row i...  31 us
    dot_general x3, matrix products, contract_cols(): lax.dot_general(left, right, (((1,), (1,)), ((), ())), preferred_element_...  29.8 us
    unnamed x143, local copies, waits for them, and re-layouts  29 us
    another operation x14, local copies, waits for them, and re-layouts, band_view(): jnp.stack([shaped[band:band + count] for band in range(PREVIOUS + 1)], ax...  27.9 us
    psum x1, blocking collectives, shards(): bias_grad = lax.psum(bias_local, 'sp')  22 us
    sub x1, other arithmetic, shards(): score_grad = weights * (prob_grad - delta)  17.5 us
  transfers between devices with their start and end apart: 7, of which 4 were waited for; matrix products, arithmetic and copies ran while one was open for 26% of the time, Pallas kernels for 0%

commit v1 on v0

v1 whole, which is shorter than its diff:
```python
import functools

import jax
import jax.numpy as jnp
from jax import lax
from jax.experimental import pallas as pl
from jax.experimental.pallas import tpu as pltpu
from jax.sharding import PartitionSpec as P

SEGMENT = 64
PREVIOUS = 4
CLIP = 256
ROWS = 2 * SEGMENT
REACH = PREVIOUS * SEGMENT
WINDOW = ROWS + REACH
TABLE = 512
HIDDEN = -1e30


def from_behind(value, axis, steps):
    count = lax.axis_size(axis)
    leading, last = (max(0, -steps), min(count, count - steps))
    return lax.ppermute(value, axis, [(source, source + steps) for source in range(leading, last)])


def contract_rows(left, right):
    return lax.dot_general(
        left, right, (((0,), (0,)), ((), ())), preferred_element_type=jnp.float32
    )


def contract_cols(left, right):
    return lax.dot_general(
        left, right, (((1,), (1,)), ((), ())), preferred_element_type=jnp.float32
    )


def diagonal_sums(tile):
    half = tile.shape[0] // 2
    while half >= 8:
        tile = tile[:half] + pltpu.roll(tile[half:], TABLE - half, 1)
        half //= 2
    row = lax.broadcasted_iota(jnp.int32, tile.shape, 0)
    for step in (4, 2, 1):
        tile = jnp.where((row & step) != 0, pltpu.roll(tile, TABLE - step, 1), tile)
    return jnp.sum(tile, axis=0, keepdims=True)


def attention_kernel(
    factor,
    first_ref,
    q_ref,
    k_ref,
    v_ref,
    pk_ref,
    pv_ref,
    g_ref,
    table_ref,
    dq_ref,
    dk_ref,
    dv_ref,
    dk_tail_ref,
    dv_tail_ref,
    dk_back_ref,
    dv_back_ref,
    table_grad_ref,
    k_all,
    v_all,
    dk_all,
    dv_all,
):
    length = q_ref.shape[0]
    k_all[:REACH] = pk_ref[...]
    k_all[REACH:] = k_ref[...]
    v_all[:REACH] = pv_ref[...]
    v_all[REACH:] = v_ref[...]
    dk_all[...] = jnp.zeros_like(dk_all)
    dv_all[...] = jnp.zeros_like(dv_all)
    first = first_ref[0]
    table = jnp.broadcast_to(table_ref[0], (ROWS, TABLE))
    bias = pltpu.roll(table, 0, 1, stride=1, stride_axis=0)[:, :WINDOW]
    row = lax.broadcasted_iota(jnp.int32, (ROWS, WINDOW), 0) // SEGMENT
    column = lax.broadcasted_iota(jnp.int32, (ROWS, WINDOW), 1)
    behind = column // SEGMENT - row
    bias = jnp.where((behind >= 0) & (behind <= PREVIOUS), bias, HIDDEN)
    bias_sum = jnp.zeros((ROWS, WINDOW), jnp.float32)
    for start in range(0, length, ROWS):
        q = q_ref[start : start + ROWS]
        g = g_ref[start : start + ROWS]
        k = k_all[start : start + WINDOW]
        v = v_all[start : start + WINDOW]
        mask = bias
        if start < REACH:
            mask = jnp.where(column + start < first, HIDDEN, bias)
        scores = contract_cols(q, k) * factor + mask
        top = jnp.max(scores, axis=1, keepdims=True)
        raised = jnp.exp(scores - top)
        weights = raised * (1.0 / jnp.sum(raised, axis=1, keepdims=True))
        prob_grad = contract_cols(g, v)
        delta = jnp.sum(weights * prob_grad, axis=1, keepdims=True)
        score_grad = weights * (prob_grad - delta)
        bias_sum = bias_sum + score_grad
        low = score_grad.astype(jnp.bfloat16)
        dq = jnp.dot(low, k, preferred_element_type=jnp.float32) * factor
        dq_ref[start : start + ROWS] = dq.astype(jnp.bfloat16)
        dk_all[start : start + WINDOW] += contract_rows(low, q)
        dv_all[start : start + WINDOW] += contract_rows(weights.astype(jnp.bfloat16), g)
    dk_back_ref[...] = (dk_all[:REACH] * factor).astype(jnp.bfloat16)
    dv_back_ref[...] = dv_all[:REACH].astype(jnp.bfloat16)
    dk_ref[...] = (dk_all[REACH:length] * factor).astype(jnp.bfloat16)
    dv_ref[...] = dv_all[REACH:length].astype(jnp.bfloat16)
    dk_tail_ref[...] = dk_all[length:] * factor
    dv_tail_ref[...] = dv_all[length:]
    padded = jnp.concatenate([bias_sum, jnp.zeros((ROWS, TABLE - WINDOW), jnp.float32)], axis=1)
    table_grad_ref[0] = diagonal_sums(padded)


def attention(query, keys, values, prev_keys, prev_values, out_grad, position_bias):
    length, width = query.shape
    heads, entries = position_bias.shape
    head = width // heads
    factor = head ** (-0.5)
    table = jnp.concatenate(
        [
            position_bias[:, ::-1],
            jnp.zeros((heads, WINDOW - entries), jnp.float32),
            jnp.broadcast_to(position_bias[:, entries - 1 :], (heads, TABLE - WINDOW)),
        ],
        axis=1,
    )[:, None]
    first = jnp.where(lax.axis_index("sp") == 0, REACH, 0).astype(jnp.int32)[None]

    def rows(count):
        return pl.BlockSpec((count, head), lambda h: (0, h))

    line = pl.BlockSpec((1, 1, TABLE), lambda h: (h, 0, 0))

    def shape(count, kind):
        return jax.ShapeDtypeStruct((count, width), kind)

    body = length - REACH
    elements = heads * length * WINDOW
    outs = pl.pallas_call(
        functools.partial(attention_kernel, factor),
        grid=(heads,),
        in_specs=[
            pl.BlockSpec(memory_space=pltpu.SMEM),
            rows(length),
            rows(length),
            rows(length),
            rows(REACH),
            rows(REACH),
            rows(length),
            line,
        ],
        out_specs=[
            rows(length),
            rows(body),
            rows(body),
            rows(REACH),
            rows(REACH),
            rows(REACH),
            rows(REACH),
            line,
        ],
        out_shape=[
            shape(length, jnp.bfloat16),
            shape(body, jnp.bfloat16),
            shape(body, jnp.bfloat16),
            shape(REACH, jnp.float32),
            shape(REACH, jnp.float32),
            shape(REACH, jnp.bfloat16),
            shape(REACH, jnp.bfloat16),
            jax.ShapeDtypeStruct((heads, 1, TABLE), jnp.float32),
        ],
        scratch_shapes=[
            pltpu.VMEM((length + REACH, head), jnp.bfloat16),
            pltpu.VMEM((length + REACH, head), jnp.bfloat16),
            pltpu.VMEM((length + REACH, head), jnp.float32),
            pltpu.VMEM((length + REACH, head), jnp.float32),
        ],
        cost_estimate=pl.CostEstimate(
            flops=10 * elements * head, bytes_accessed=14 * length * width, transcendentals=elements
        ),
    )(first, query, keys, values, prev_keys, prev_values, out_grad, table)
    return outs


def table_to_bias(summed, entries):
    near = summed[:, 1:entries][:, ::-1]
    far = summed[:, :1] + jnp.sum(summed[:, WINDOW:], axis=1, keepdims=True)
    return jnp.concatenate([near, far], axis=1)


def shards(tokens, query_weight, key_weight, value_weight, position_bias, out_grad):
    whole = lax.all_gather(tokens, "tp", axis=1, tiled=True)
    keys = jnp.dot(whole, key_weight, preferred_element_type=jnp.float32).astype(jnp.bfloat16)
    values = jnp.dot(whole, value_weight, preferred_element_type=jnp.float32).astype(jnp.bfloat16)
    length = keys.shape[0]
    prev_keys, prev_values = from_behind(
        (keys[length - REACH :], values[length - REACH :]), "sp", 1
    )
    query = jnp.dot(whole, query_weight, preferred_element_type=jnp.float32).astype(jnp.bfloat16)
    query_grad, key_body, value_body, key_tail, value_tail, key_back, value_back, lines = attention(
        query, keys, values, prev_keys, prev_values, out_grad, position_bias
    )
    key_next, value_next = from_behind((key_back, value_back), "sp", -1)

    def scatter(grad):
        part = contract_rows(whole, grad).astype(jnp.bfloat16)
        return lax.psum_scatter(part, "sp", scatter_dimension=0, tiled=True).astype(jnp.float32)

    query_weight_grad = scatter(query_grad)
    value_grad = jnp.concatenate([value_body, (value_tail + value_next).astype(jnp.bfloat16)])
    value_weight_grad = scatter(value_grad)
    key_grad = jnp.concatenate([key_body, (key_tail + key_next).astype(jnp.bfloat16)])
    key_weight_grad = scatter(key_grad)
    input_part = (
        contract_cols(query_grad, query_weight)
        + contract_cols(key_grad, key_weight)
        + contract_cols(value_grad, value_weight)
    )
    input_grad = lax.psum_scatter(
        input_part.astype(jnp.bfloat16), "tp", scatter_dimension=1, tiled=True
    )
    bias_grad = table_to_bias(lax.psum(lines[:, 0], "sp"), position_bias.shape[1])
    return input_grad, query_weight_grad, key_weight_grad, value_weight_grad, bias_grad


def solution(mesh):
    in_specs = (
        P("sp", "tp"),
        P(None, "tp"),
        P(None, "tp"),
        P(None, "tp"),
        P("tp", None),
        P("sp", "tp"),
    )
    out_specs = (P("sp", "tp"), P("sp", "tp"), P("sp", "tp"), P("sp", "tp"), P("tp", None))
    return jax.shard_map(shards, mesh=mesh, in_specs=in_specs, out_specs=out_specs, check_vma=False)
```

time: 693 us -> 456 us (0.66)
  waiting for transfers between devices: 432 us -> 299 us
  local copies, waits for them, and re-layouts: 110 us -> 14.5 us
  other arithmetic: 29.4 us -> 0.96 us
  Pallas kernels: 0 us -> 17.2 us
  blocking collectives: 22 us -> 30.2 us
    reduce_scatter x1 -> x3, waiting for transfers between devices: 351 us -> 168 us  [scatter(): lax.psum_scatter(part, 'sp', scatter_dimension=0, tiled=True)]
    another operation x83 -> x0, local copies, waits for them, and re-layouts: 58.9 us -> none  [the longest x69 31 us: shards(): jnp.stack([along[:, SEGMENT - 1 - row:SEGMENT - 1 - row + span] for row i...]
    all_gather x1, waiting for transfers between devices: 15.9 us -> 47.5 us  [shards(): whole = lax.all_gather(tokens, 'tp', axis=1, tiled=True)]
    sub x1 -> x0, other arithmetic: 17.5 us -> none  [shards(): score_grad = weights * (prob_grad - delta)]
    pallas_call x0 -> x1, Pallas kernels: none -> 17.2 us  [attention(): pl.pallas_call(functools.partial(attention_kernel, factor), grid=(heads,)...]
    unnamed x143 -> x40, local copies, waits for them, and re-layouts: 29 us -> 12.6 us
    ppermute x4, waiting for transfers between devices: 10.7 us -> 24.9 us  [from_behind(): lax.ppermute(value, axis, [(source, source + steps) for source in range(l...]
    dot_general x1 -> x3, matrix products: 13.9 us -> 24.2 us  [contract_rows(): lax.dot_general(left, right, (((0,), (0,)), ((), ())), preferred_element_...]
  transfers between devices with their start and end apart: 7 -> 9, of which waited for: 4 -> 7; matrix products, arithmetic and copies ran while one was open for 26% -> 14% of each run, Pallas kernels for 0% -> 0%
where the time goes in v1:
time: 456 us; the launch traced here: 455 us
  waiting for transfers between devices  299 us (66%)
  matrix products  69.1 us (15%)
  blocking collectives  30.2 us (7%)
  Pallas kernels  17.2 us (4%)
  local copies, waits for them, and re-layouts  14.5 us (3%)
  between operations  14 us (3%)
  starting transfers between devices  10.2 us (2%)
    reduce_scatter x3, waiting for transfers between devices, scatter(): lax.psum_scatter(part, 'sp', scatter_dimension=0, tiled=True)  168 us
    reduce_scatter x1, waiting for transfers between devices, shards(): lax.psum_scatter(input_part.astype(jnp.bfloat16), 'tp', scatter_dimension...  58.3 us
    all_gather x1, waiting for transfers between devices, shards(): whole = lax.all_gather(tokens, 'tp', axis=1, tiled=True)  47.5 us
    psum x1, blocking collectives, shards(): lax.psum(lines[:, 0], 'sp')  30.2 us
    dot_general x3, matrix products, contract_cols(): lax.dot_general(left, right, (((1,), (1,)), ((), ())), preferred_element_...  29.7 us
    ppermute x4, waiting for transfers between devices, from_behind(): lax.ppermute(value, axis, [(source, source + steps) for source in range(l...  24.9 us
    dot_general x3, matrix products, contract_rows(): lax.dot_general(left, right, (((0,), (0,)), ((), ())), preferred_element_...  24.2 us
    pallas_call x1, Pallas kernels, attention(): pl.pallas_call(functools.partial(attention_kernel, factor), grid=(heads,)...  17.2 us
  transfers between devices with their start and end apart: 9, of which 7 were waited for; matrix products, arithmetic and copies ran while one was open for 14% of the time, Pallas kernels for 0%

profile of v1, /device:TPU:0, one launch (start us, length us, event | category | flops | bytes accessed | tf_op | source)
XLA Modules:
  0.0 455.3 jit_solution(9533891556518814449)
XLA Ops:
  7.2 0.0 all-gather.2.cloned.1.call-start
  7.2 0.7 all-gather.2.cloned.1.call-update
  7.9 0.0 reduce-scatter.7.cloned.1.call-start
  7.9 1.5 reverse
  9.5 0.1 slice.32
  9.6 0.1 pad.7.clone
  9.6 0.9 slice_reduce_fusion.1
  10.5 0.1 broadcast_in_dim.22
  10.6 0.6 broadcast_in_dim.23.table_ref
  11.2 47.5 %all-gather.2.cloned.1.call-done = bf16[768,4096]{1,0:T(8,128)(2,1)} async-done(((bf16[768,1024]{1,0:T(8,128)(2,1)}), bf16[768,4096]{1,0:T(8,128)(2,1)}) %all-gather.2.cloned.1.call-update) | async-done | bytes 6291472 | tf_op jit(solution)/shard_map/all_gather | solution.py:196
  58.7 7.6 %convolution_convert_fusion.3.v_ref = bf16[768,512]{1,0:T(8,128)(2,1)S(1)} fusion(bf16[768,4096]{1,0:T(8,128)(2,1)} %all-gather.2.cloned.1.call-done, bf16[4096,512]{1,0:T(8,128)(2,1)} %param.9), kind=kOutput, calls=%fused_computation.7 | convolution fusion | flops 3221618688 | bytes 11272192 | tf_op jit(solution)/shard_map/dot_general | solution.py:198
  66.2 0.0 copy-start.3
  66.3 0.0 copy-start.7
  66.3 3.6 collective-permute-start.1
  69.9 0.0 copy-done.6
  69.9 0.0 copy-done.8
  69.9 3.4 convolution_convert_fusion.4.k_ref
  73.3 0.0 copy-done.3
  73.4 0.0 copy-start.4
  73.4 3.6 collective-permute-start
  77.0 0.0 copy-done.7
  77.0 4.3 convolution_convert_fusion.5.q_ref
  81.3 0.0 collective-permute-done.1.pv_ref
  81.3 1.2 collective-permute-done.pk_ref
  82.5 0.0 copy-done.12
  82.5 0.7 copy-done.13
  83.2 17.2 %shard_map.101 = (bf16[768,512]{1,0:T(8,128)(2,1)}, bf16[512,512]{1,0:T(8,128)(2,1)}, bf16[512,512]{1,0:T(8,128)(2,1)}, f32[256,512]{1,0:T(8,128)}, f32[256,512]...) custom-call(s32[1]{0:T(128)} %bitcast.first_ref, ...), custom_call_target="tpu_custom_call" | custom-call | flops 1509949440 | bytes 5505024 | tf_op jit(solution)/shard_map/pallas_call | solution.py:143
  100.4 8.5 %fusion = bf16[4096,512]{0,1:T(8,128)(2,1)} fusion(bf16[768,512]{1,0:T(8,128)(2,1)} %get-tuple-element.13, bf16[768,4096]{1,0:T(8,128)(2,1)} %all-gather.2.cloned.1.call-done), kind=kOutput, calls=%fused_computation.4 | convolution fusion | flops 3223322624 | bytes 11272192 | tf_op jit(solution)/shard_map/dot_general | solution.py:27
  108.9 0.0 reduce-scatter.7.cloned.1.call-update
  108.9 0.0 reduce-scatter.11.cloned.1.call-start
  108.9 0.9 copy-done.11
  109.8 1.3 collective-permute-start.3
  111.1 9.8 %collective-permute-done.3 = bf16[256,512]{1,0:T(8,128)(2,1)S(1)} collective-permute-done((bf16[256,512]{1,0:T(8,128)(2,1)S(1)}, bf16[256,512]{1,0:T(8,128)(2,1)S(1)}, u32[]{:S(2)}, u32[]{:S(2)}) %collective-permute-start.3) | collective-permute-done | bytes 262176 | tf_op jit(solution)/shard_map/ppermute | solution.py:23
  120.9 0.1 add_convert_fusion.1
  121.0 0.0 copy-done
  121.0 7.8 %fusion.2 = bf16[4096,512]{0,1:T(8,128)(2,1)} fusion(bf16[768,4096]{1,0:T(8,128)(2,1)} %all-gather.2.cloned.1.call-done, bf16[256,512]{1,0:T(8,128)(2,1)S(1)} %add_convert_fusion.1, bf16[512,512]{1,0:T(8,128)(2,1)S(1)} %copy-done), kind=kOutput, calls=%fused_computation.6 | convolution fusion | flops 3224895488 | bytes 11272192 | tf_op jit(solution)/shard_map/dot_general | solution.py:27
  128.8 0.0 reduce-scatter.11.cloned.1.call-update
  128.8 0.0 reduce-scatter.9.cloned.1.call-start
  128.9 0.9 copy-done.10
  129.8 1.3 collective-permute-start.2
  131.0 13.9 %collective-permute-done.2 = bf16[256,512]{1,0:T(8,128)(2,1)S(1)} collective-permute-done((bf16[256,512]{1,0:T(8,128)(2,1)S(1)}, bf16[256,512]{1,0:T(8,128)(2,1)S(1)}, u32[]{:S(2)}, u32[]{:S(2)}) %collective-permute-start.2) | collective-permute-done | bytes 262176 | tf_op jit(solution)/shard_map/ppermute | solution.py:23
  144.9 0.1 add_convert_fusion.2
  145.0 7.9 %fusion.1 = bf16[4096,512]{0,1:T(8,128)(2,1)} fusion(bf16[768,4096]{1,0:T(8,128)(2,1)} %all-gather.2.cloned.1.call-done, bf16[256,512]{1,0:T(8,128)(2,1)S(1)} %add_convert_fusion.2, bf16[512,512]{1,0:T(8,128)(2,1)S(1)} %copy-done.15), kind=kOutput, calls=%fused_computation.5 | convolution fusion | flops 3224895488 | bytes 11272192 | tf_op jit(solution)/shard_map/dot_general | solution.py:27
  152.9 0.0 reduce-scatter.9.cloned.1.call-update
  152.9 0.3 reduce-scatter.5.cloned.1.call-start
  153.2 0.8 copy-done.14
  154.0 8.8 %fusion.9 = f32[768,4096]{1,0:T(8,128)} fusion(bf16[768,512]{1,0:T(8,128)(2,1)S(1)} %copy-done.14, bf16[4096,512]{1,0:T(8,128)(2,1)} %param.7), kind=kOutput, calls=%fused_computation.26 | convolution fusion | flops 3221225472 | bytes 17563648 | tf_op jit(solution)/shard_map/dot_general | solution.py:33
  162.9 6.5 %fusion.4 = f32[768,4096]{1,0:T(8,128)} fusion(bf16[4096,512]{1,0:T(8,128)(2,1)S(1)} %copy-done.9, bf16[256,512]{1,0:T(8,128)(2,1)S(1)} %add_convert_fusion.2, bf16[512,512]{1,0:T(8,128)(2,1)S(1)} %copy-done.15), kind=kOutput, calls=%fused_computation.15 | convolution fusion | flops 3222798336 | bytes 17563648 | tf_op jit(solution)/shard_map/dot_general | solution.py:33
  169.4 14.4 %add_convert_fusion = bf16[768,4096]{1,0:T(8,128)(2,1)} fusion(f32[768,4096]{1,0:T(8,128)} %fusion.9, f32[768,4096]{1,0:T(8,128)} %fusion.4, bf16[4096,512]{1,0:T(8,128)(2,1)} %param.9, bf16[256,512]{1,0:T(8,128)(2,1)S(1)} %add_convert_fusion.1, bf16[512,512]{1,0:T(8,128)(2,1)S(1)} %copy-done), kind=kOutput, calls=%fused_computation | convolution fusion | flops 3232235520 | bytes 36438016 | tf_op jit(solution)/shard_map/dot_general | solution.py:33
  183.8 0.0 reduce-scatter.5.cloned.1.call-update
  183.8 0.7 copy-done.5
  184.5 30.2 %psum.7 = f32[4,512]{1,0:T(4,128)S(1)} all-reduce(f32[4,512]{1,0:T(4,128)S(1)} %bitcast.27), channel_id=1, replica_groups=mesh['sp'=8,'tp'=4] {'sp'}, use_global_device_ids=true, to_apply=%region_4.5 | all-reduce | flops 2048 | bytes 16384 | tf_op jit(solution)/shard_map/psum | solution.py:226
  214.7 0.1 slice.26
  214.8 0.1 slice_reduce_fusion
  214.9 0.1 copy.11
  215.0 0.3 reverse.1
  215.3 0.1 slice.33
  215.3 0.7 pad_maximum_fusion.9
  216.0 2.2 copy.12
  218.2 78.2 %reduce-scatter.11.cloned.1.call-done = bf16[512,512]{0,1:T(8,128)(2,1)} async-done(((bf16[4096,512]{0,1:T(8,128)(2,1)}), bf16[512,512]{0,1:T(8,128)(2,1)}) %reduce-scatter.11.cloned.1.call-update) | async-done | bytes 524304 | tf_op jit(solution)/shard_map/reduce_scatter | solution.py:211
  296.4 2.2 copy.14
  298.7 89.6 %reduce-scatter.9.cloned.1.call-done = bf16[512,512]{0,1:T(8,128)(2,1)} async-done(((bf16[4096,512]{0,1:T(8,128)(2,1)}), bf16[512,512]{0,1:T(8,128)(2,1)}) %reduce-scatter.9.cloned.1.call-update) | async-done | bytes 524304 | tf_op jit(solution)/shard_map/reduce_scatter | solution.py:211
  388.3 2.2 copy.13
  390.5 58.3 %reduce-scatter.5.cloned.1.call-done = bf16[768,1024]{1,0:T(8,128)(2,1)} async-done(((bf16[768,4096]{1,0:T(8,128)(2,1)}), bf16[768,1024]{1,0:T(8,128)(2,1)}) %reduce-scatter.5.cloned.1.call-update) | async-done | bytes 1572880 | tf_op jit(solution)/shard_map/reduce_scatter | solution.py:223
  (25 shorter events, 0.1 us)
Async XLA Ops:
  7.2 51.5 %all-gather.2.cloned.1.call-start = ((), (), s32[]{:S(2)}) async-start(), calls=%async_computation.4 | async-start | bytes 7864320 | tf_op jit(solution)/shard_map/all_gather | solution.py:196
  7.9 208.1 %reduce-scatter.7.cloned.1.call-start = ((), (), s32[]{:S(2)}) async-start(), calls=%async_computation.6 | async-start | bytes 4718592 | tf_op jit(solution)/shard_map/reduce_scatter | solution.py:211
  58.7 11.3 %copy-start.6 = (bf16[768,4096]{1,0:T(8,128)(2,1)S(1)}, bf16[768,4096]{1,0:T(8,128)(2,1)}, u32[]{:S(2)}) copy-start(bf16[768,4096]{1,0:T(8,128)(2,1)} %all-gather.2.cloned.1.call-done) | copy-start | bytes 18874372
  58.7 11.3 %copy-start.8 = (bf16[4096,512]{1,0:T(8,128)(2,1)S(1)}, bf16[4096,512]{1,0:T(8,128)(2,1)}, u32[]{:S(2)}) copy-start(bf16[4096,512]{1,0:T(8,128)(2,1)} %param.8) | copy-start | bytes 12582916
  66.2 7.1 %copy-start.3 = (bf16[768,512]{1,0:T(8,128)(2,1)}, bf16[768,512]{1,0:T(8,128)(2,1)S(1)}, u32[]{:S(2)}) copy-start(bf16[768,512]{1,0:T(8,128)(2,1)S(1)} %convolution_convert_fusion.3.v_ref) | copy-start | bytes 2359300
  66.3 10.7 %copy-start.7 = (bf16[4096,512]{1,0:T(8,128)(2,1)S(1)}, bf16[4096,512]{1,0:T(8,128)(2,1)}, u32[]{:S(2)}) copy-start(bf16[4096,512]{1,0:T(8,128)(2,1)} %param.7) | copy-start | bytes 12582916
  66.3 15.0 %collective-permute-start.1 = (bf16[256,512]{1,0:T(8,128)(2,1)S(1)}, bf16[256,512]{1,0:T(8,128)(2,1)S(1)}, u32[]{:S(2)}, u32[]{:S(2)}) collective-permute-start(bf16[256,512]{1,0:T(8,128)(2,1)S(1)} %slice.25), channel_id=1, source_target_pairs={{0,4},{4,8},{8,12},{12,16},{16,20},{20,24},{24,28},{1,5},{5,9},{9,... | collective-permute-start | bytes 786440 | tf_op jit(solution)/shard_map/ppermute | solution.py:23
  73.4 7.9 %copy-start.4 = (bf16[768,512]{1,0:T(8,128)(2,1)}, bf16[768,512]{1,0:T(8,128)(2,1)S(1)}, u32[]{:S(2)}) copy-start(bf16[768,512]{1,0:T(8,128)(2,1)S(1)} %convolution_convert_fusion.4.k_ref) | copy-start | bytes 2359300
  73.4 9.1 %collective-permute-start = (bf16[256,512]{1,0:T(8,128)(2,1)S(1)}, bf16[256,512]{1,0:T(8,128)(2,1)S(1)}, u32[]{:S(2)}, u32[]{:S(2)}) collective-permute-start(bf16[256,512]{1,0:T(8,128)(2,1)S(1)} %slice.24), channel_id=1, source_target_pairs={{0,4},{4,8},{8,12},{12,16},{16,20},{20,24},{24,28},{1,5},{5,9},{9,... | collective-permute-start | bytes 786440 | tf_op jit(solution)/shard_map/ppermute | solution.py:23
  81.3 1.2 copy-start.12
  82.5 0.7 copy-start.13
  108.9 0.9 copy-start.11
  108.9 12.0 %copy-start.2 = (f32[256,512]{1,0:T(8,128)S(1)}, f32[256,512]{1,0:T(8,128)}, u32[]{:S(2)}) copy-start(f32[256,512]{1,0:T(8,128)} %get-tuple-element.18) | copy-start | bytes 1572868
  108.9 12.1 %copy-start = (bf16[512,512]{1,0:T(8,128)(2,1)S(1)}, bf16[512,512]{1,0:T(8,128)(2,1)}, u32[]{:S(2)}) copy-start(bf16[512,512]{1,0:T(8,128)(2,1)} %get-tuple-element.17) | copy-start | bytes 1572868
  108.9 187.6 %reduce-scatter.11.cloned.1.call-start = ((), (), s32[]{:S(2)}) async-start(), calls=%async_computation.8 | async-start | bytes 4718592 | tf_op jit(solution)/shard_map/reduce_scatter | solution.py:211
  109.8 11.1 %collective-permute-start.3 = (bf16[256,512]{1,0:T(8,128)(2,1)S(1)}, bf16[256,512]{1,0:T(8,128)(2,1)S(1)}, u32[]{:S(2)}, u32[]{:S(2)}) collective-permute-start(bf16[256,512]{1,0:T(8,128)(2,1)S(1)} %copy-done.11), channel_id=1, source_target_pairs={{4,0},{8,4},{12,8},{16,12},{20,16},{24,20},{28,24},{5,1},{9,5},{13... | collective-permute-start | bytes 786440 | tf_op jit(solution)/shard_map/ppermute | solution.py:23
  128.8 1.0 copy-start.10
  128.8 16.1 %copy-start.1 = (f32[256,512]{1,0:T(8,128)S(1)}, f32[256,512]{1,0:T(8,128)}, u32[]{:S(2)}) copy-start(f32[256,512]{1,0:T(8,128)} %get-tuple-element.15) | copy-start | bytes 1572868
  128.8 16.2 %copy-start.15 = (bf16[512,512]{1,0:T(8,128)(2,1)S(1)}, bf16[512,512]{1,0:T(8,128)(2,1)}, u32[]{:S(2)}) copy-start(bf16[512,512]{1,0:T(8,128)(2,1)} %get-tuple-element.14) | copy-start | bytes 1572868
  128.8 259.5 %reduce-scatter.9.cloned.1.call-start = ((), (), s32[]{:S(2)}) async-start(), calls=%async_computation.7 | async-start | bytes 4718592 | tf_op jit(solution)/shard_map/reduce_scatter | solution.py:211
  129.8 15.1 %collective-permute-start.2 = (bf16[256,512]{1,0:T(8,128)(2,1)S(1)}, bf16[256,512]{1,0:T(8,128)(2,1)S(1)}, u32[]{:S(2)}, u32[]{:S(2)}) collective-permute-start(bf16[256,512]{1,0:T(8,128)(2,1)S(1)} %copy-done.10), channel_id=1, source_target_pairs={{4,0},{8,4},{12,8},{16,12},{20,16},{24,20},{28,24},{5,1},{9,5},{13... | collective-permute-start | bytes 786440 | tf_op jit(solution)/shard_map/ppermute | solution.py:23
  152.9 1.1 copy-start.14
  152.9 295.9 %reduce-scatter.5.cloned.1.call-start = ((), (), s32[]{:S(2)}) async-start(), calls=%async_computation.5 | async-start | bytes 7864320 | tf_op jit(solution)/shard_map/reduce_scatter | solution.py:223
  154.0 8.9 %copy-start.9 = (bf16[4096,512]{1,0:T(8,128)(2,1)S(1)}, bf16[4096,512]{1,0:T(8,128)(2,1)}, u32[]{:S(2)}) copy-start(bf16[4096,512]{1,0:T(8,128)(2,1)} %param.8) | copy-start | bytes 12582916
  183.8 0.7 copy-start.5
Sparse Core Ops, SparseCore 0:
  9.5 49.0 all-gather.1
  109.0 95.1 reduce-scatter.6
  207.9 88.5 reduce-scatter.10
  299.9 88.3 reduce-scatter.8
  391.2 57.5 reduce-scatter.4

commit v2 on v1

--- a/solution.py
+++ b/solution.py
@@ -61,8 +61,7 @@
     dv_ref,
     dk_tail_ref,
     dv_tail_ref,
-    dk_back_ref,
-    dv_back_ref,
+    back_ref,
     table_grad_ref,
     k_all,
     v_all,
@@ -105,8 +104,8 @@
         dq_ref[start : start + ROWS] = dq.astype(jnp.bfloat16)
         dk_all[start : start + WINDOW] += contract_rows(low, q)
         dv_all[start : start + WINDOW] += contract_rows(weights.astype(jnp.bfloat16), g)
-    dk_back_ref[...] = (dk_all[:REACH] * factor).astype(jnp.bfloat16)
-    dv_back_ref[...] = dv_all[:REACH].astype(jnp.bfloat16)
+    back_ref[0] = (dk_all[:REACH] * factor).astype(jnp.bfloat16)
+    back_ref[1] = dv_all[:REACH].astype(jnp.bfloat16)
     dk_ref[...] = (dk_all[REACH:length] * factor).astype(jnp.bfloat16)
     dv_ref[...] = dv_all[REACH:length].astype(jnp.bfloat16)
     dk_tail_ref[...] = dk_all[length:] * factor
@@ -159,8 +158,7 @@
             rows(body),
             rows(REACH),
             rows(REACH),
-            rows(REACH),
-            rows(REACH),
+            pl.BlockSpec((2, REACH, head), lambda h: (0, 0, h)),
             line,
         ],
         out_shape=[
@@ -169,8 +167,7 @@
             shape(body, jnp.bfloat16),
             shape(REACH, jnp.float32),
             shape(REACH, jnp.float32),
-            shape(REACH, jnp.bfloat16),
-            shape(REACH, jnp.bfloat16),
+            jax.ShapeDtypeStruct((2, REACH, width), jnp.bfloat16),
             jax.ShapeDtypeStruct((heads, 1, TABLE), jnp.float32),
         ],
         scratch_shapes=[
@@ -192,7 +189,164 @@
     return jnp.concatenate([near, far], axis=1)
 
 
+def ring_columns(count):
+    columns = 1
+    while (2 * columns) ** 2 <= count:
+        columns *= 2
+    return columns
+
+
+def ring_place(index, count):
+    columns = ring_columns(count)
+    rows = count // columns
+    row, column = index // columns, index % columns
+    above = rows - 1 - row
+    across = jnp.where(above % 2 == 0, column - 1, columns - 1 - column)
+    return jnp.where(column == 0, row, rows + above * (columns - 1) + across)
+
+
+def ring_index(place, count):
+    columns = ring_columns(count)
+    rows = count // columns
+    later = jnp.maximum(place - rows, 0)
+    above, across = later // (columns - 1), later % (columns - 1)
+    column = jnp.where(above % 2 == 0, 1 + across, columns - 1 - across)
+    return jnp.where(place < rows, place * columns, (rows - 1 - above) * columns + column)
+
+
+def ring_kernel(
+    count,
+    whole_ref,
+    dq_ref,
+    dk_ref,
+    dv_ref,
+    line_ref,
+    oq_ref,
+    ok_ref,
+    ov_ref,
+    line_out_ref,
+    sent,
+    got,
+    lines,
+    send_sem,
+    recv_sem,
+    line_send,
+    line_recv,
+):
+    me = lax.axis_index("sp")
+    place = ring_place(me, count)
+    barrier = pltpu.get_barrier_semaphore()
+    for ahead in range(1, count):
+        peer = lax.rem(me + ahead, count)
+        pl.semaphore_signal(
+            barrier, inc=1, device_id={"sp": peer}, device_id_type=pl.DeviceIdType.MESH
+        )
+    pl.semaphore_wait(barrier, count - 1)
+
+    grads = (dq_ref, dk_ref, dv_ref)
+    outs = (oq_ref, ok_ref, ov_ref)
+    half = sent.shape[3]
+    onward = (
+        ring_index(lax.rem(place + 1, count), count),
+        ring_index(lax.rem(place + count - 1, count), count),
+    )
+
+    def own(target, side, chain):
+        start = pl.multiple_of((2 * ring_index(target, count) + side) * half, half)
+        return contract_rows(whole_ref[:, pl.ds(start, half)], grads[chain][...])
+
+    def target_of(step, side):
+        if side == 0:
+            return lax.rem(place - 1 - step + 2 * count, count)
+        return lax.rem(place + 1 + step, count)
+
+    def copy_of(step, side, chain):
+        return pltpu.make_async_remote_copy(
+            src_ref=sent.at[side, chain, step],
+            dst_ref=got.at[side, chain, step],
+            send_sem=send_sem.at[side, chain, step],
+            recv_sem=recv_sem.at[side, chain, step],
+            device_id={"sp": onward[side]},
+            device_id_type=pl.DeviceIdType.MESH,
+        )
+
+    def line_copy(ahead):
+        return pltpu.make_async_remote_copy(
+            src_ref=line_ref,
+            dst_ref=lines.at[ahead - 1],
+            send_sem=line_send.at[ahead - 1],
+            recv_sem=line_recv.at[ahead - 1],
+            device_id={"sp": lax.rem(me + ahead, count)},
+            device_id_type=pl.DeviceIdType.MESH,
+        )
+
+    chains = [(chain, side) for chain in range(3) for side in range(2)]
+    for chain, side in chains:
+        sent[side, chain, 0] = own(target_of(0, side), side, chain).astype(jnp.bfloat16)
+        copy_of(0, side, chain).start()
+    for ahead in range(1, count):
+        line_copy(ahead).start()
+
+    @pl.loop(1, count - 1)
+    def _(step):
+        for chain, side in chains:
+            part = own(target_of(step, side), side, chain)
+            copy_of(step - 1, side, chain).wait_recv()
+            total = part + got[side, chain, step - 1].astype(jnp.float32)
+            sent[side, chain, step] = total.astype(jnp.bfloat16)
+            copy_of(step, side, chain).start()
+
+    total = line_ref[...]
+    for ahead in range(1, count):
+        line_copy(ahead).wait()
+        total = total + lines[ahead - 1]
+    line_out_ref[...] = total
+    for chain, side in chains:
+        part = own(place, side, chain)
+        copy_of(count - 2, side, chain).wait_recv()
+        total = part + got[side, chain, count - 2].astype(jnp.float32)
+        outs[chain][side * half : (side + 1) * half] = total
+
+    @pl.loop(0, count - 1)
+    def _(step):
+        for chain, side in chains:
+            copy_of(step, side, chain).wait_send()
+
+
+def weight_grads(whole, query_grad, key_grad, value_grad, lines):
+    count = lax.axis_size("sp")
+    features = whole.shape[1]
+    width = query_grad.shape[1]
+    half = features // count // 2
+    vmem = pl.BlockSpec(memory_space=pltpu.VMEM)
+    out = jax.ShapeDtypeStruct((2 * half, width), jnp.float32)
+    return pl.pallas_call(
+        functools.partial(ring_kernel, count),
+        in_specs=[vmem] * 5,
+        out_specs=[vmem] * 4,
+        out_shape=[out, out, out, jax.ShapeDtypeStruct(lines.shape, jnp.float32)],
+        scratch_shapes=[
+            pltpu.VMEM((2, 3, count - 1, half, width), jnp.bfloat16),
+            pltpu.VMEM((2, 3, count - 1, half, width), jnp.bfloat16),
+            pltpu.VMEM((count - 1,) + lines.shape, jnp.float32),
+            pltpu.SemaphoreType.DMA((2, 3, count - 1)),
+            pltpu.SemaphoreType.DMA((2, 3, count - 1)),
+            pltpu.SemaphoreType.DMA((count - 1,)),
+            pltpu.SemaphoreType.DMA((count - 1,)),
+        ],
+        compiler_params=pltpu.CompilerParams(
+            collective_id=0, has_side_effects=True, vmem_limit_bytes=56 * 1024 * 1024
+        ),
+        cost_estimate=pl.CostEstimate(
+            flops=6 * whole.shape[0] * features * width,
+            bytes_accessed=400_000_000,
+            transcendentals=0,
+        ),
+    )(whole, query_grad, key_grad, value_grad, lines)
+
+
 def shards(tokens, query_weight, key_weight, value_weight, position_bias, out_grad):
+    weights = jnp.concatenate([query_weight, key_weight, value_weight], axis=1)
     whole = lax.all_gather(tokens, "tp", axis=1, tiled=True)
     keys = jnp.dot(whole, key_weight, preferred_element_type=jnp.float32).astype(jnp.bfloat16)
     values = jnp.dot(whole, value_weight, preferred_element_type=jnp.float32).astype(jnp.bfloat16)
@@ -201,29 +355,20 @@
         (keys[length - REACH :], values[length - REACH :]), "sp", 1
     )
     query = jnp.dot(whole, query_weight, preferred_element_type=jnp.float32).astype(jnp.bfloat16)
-    query_grad, key_body, value_body, key_tail, value_tail, key_back, value_back, lines = attention(
+    query_grad, key_body, value_body, key_tail, value_tail, back, lines = attention(
         query, keys, values, prev_keys, prev_values, out_grad, position_bias
     )
-    key_next, value_next = from_behind((key_back, value_back), "sp", -1)
-
-    def scatter(grad):
-        part = contract_rows(whole, grad).astype(jnp.bfloat16)
-        return lax.psum_scatter(part, "sp", scatter_dimension=0, tiled=True).astype(jnp.float32)
-
-    query_weight_grad = scatter(query_grad)
-    value_grad = jnp.concatenate([value_body, (value_tail + value_next).astype(jnp.bfloat16)])
-    value_weight_grad = scatter(value_grad)
-    key_grad = jnp.concatenate([key_body, (key_tail + key_next).astype(jnp.bfloat16)])
-    key_weight_grad = scatter(key_grad)
-    input_part = (
-        contract_cols(query_grad, query_weight)
-        + contract_cols(key_grad, key_weight)
-        + contract_cols(value_grad, value_weight)
-    )
-    input_grad = lax.psum_scatter(
-        input_part.astype(jnp.bfloat16), "tp", scatter_dimension=1, tiled=True
-    )
-    bias_grad = table_to_bias(lax.psum(lines[:, 0], "sp"), position_bias.shape[1])
+    after = from_behind(back, "sp", -1)
+    key_grad = jnp.concatenate([key_body, (key_tail + after[0]).astype(jnp.bfloat16)])
+    value_grad = jnp.concatenate([value_body, (value_tail + after[1]).astype(jnp.bfloat16)])
+    grads = jnp.concatenate([query_grad, key_grad, value_grad], axis=1)
+    input_part = contract_cols(grads, weights).astype(jnp.bfloat16)
+    input_grad = lax.psum_scatter(input_part, "tp", scatter_dimension=1, tiled=True)
+    barrier = lax.optimization_barrier((key_grad, input_part))
+    query_weight_grad, key_weight_grad, value_weight_grad, lines = weight_grads(
+        whole, query_grad, barrier[0], value_grad, lines[:, 0]
+    )
+    bias_grad = table_to_bias(lines, position_bias.shape[1])
     return input_grad, query_weight_grad, key_weight_grad, value_weight_grad, bias_grad
 
 

time: 456 us -> 282 us (0.62)
  waiting for transfers between devices: 299 us -> 63.8 us
  Pallas kernels: 17.2 us -> 148 us
  matrix products: 69.1 us -> 30.5 us
  blocking collectives: 30.2 us -> 0 us
    reduce_scatter x4 -> x1, waiting for transfers between devices: 226 us -> 0.01 us  [shards(): lax.psum_scatter(input_part, 'tp', scatter_dimension=1, tiled=True)]
    pallas_call x0 -> x1, Pallas kernels: none -> 131 us  [weight_grads(): pl.pallas_call(functools.partial(ring_kernel, count), in_specs=[vmem] * 5...]
    psum x1 -> x0, blocking collectives: 30.2 us -> none  [shards(): lax.psum(lines[:, 0], 'sp')]
    dot_general x3 -> x0, matrix products: 24.2 us -> none  [contract_rows(): lax.dot_general(left, right, (((0,), (0,)), ((), ())), preferred_element_...]
    dot_general x3 -> x1, matrix products: 29.7 us -> 15.2 us  [contract_cols(): lax.dot_general(left, right, (((1,), (1,)), ((), ())), preferred_element_...]
    ppermute x4 -> x3, waiting for transfers between devices: 24.9 us -> 15.7 us  [from_behind(): lax.ppermute(value, axis, [(source, source + steps) for source in range(l...]
    unnamed x40 -> x30, local copies, waits for them, and re-layouts: 12.6 us -> 9.47 us
    ppermute x4 -> x3, starting transfers between devices: 9.77 us -> 8.51 us  [from_behind(): lax.ppermute(value, axis, [(source, source + steps) for source in range(l...]
  transfers between devices with their start and end apart: 9 -> 5, of which waited for: 7 -> 3; matrix products, arithmetic and copies ran while one was open for 14% -> 6% of each run, Pallas kernels for 0% -> 46%
where the time goes in v2:
time: 282 us
  Pallas kernels  148 us (52%)
  waiting for transfers between devices  63.8 us (23%)
  matrix products  30.5 us (11%)
  between operations  14.2 us (5%)
  local copies, waits for them, and re-layouts  12.1 us (4%)
  starting transfers between devices  8.58 us (3%)
  other arithmetic  4.73 us (2%)
    pallas_call x1, Pallas kernels, weight_grads(): pl.pallas_call(functools.partial(ring_kernel, count), in_specs=[vmem] * 5...  131 us
    all_gather x1, waiting for transfers between devices, shards(): whole = lax.all_gather(tokens, 'tp', axis=1, tiled=True)  47.5 us
    pallas_call x1, Pallas kernels, attention(): pl.pallas_call(functools.partial(attention_kernel, factor), grid=(heads,)...  17.2 us
    ppermute x3, waiting for transfers between devices, from_behind(): lax.ppermute(value, axis, [(source, source + steps) for source in range(l...  15.7 us
    dot_general x1, matrix products, contract_cols(): lax.dot_general(left, right, (((1,), (1,)), ((), ())), preferred_element_...  15.2 us
    unnamed x30, local copies, waits for them, and re-layouts  9.47 us
    ppermute x3, starting transfers between devices, from_behind(): lax.ppermute(value, axis, [(source, source + steps) for source in range(l...  8.51 us
    dot_general x1, matrix products, shards(): jnp.dot(whole, key_weight, preferred_element_type=jnp.float32)  7.55 us
  transfers between devices with their start and end apart: 5, of which 3 were waited for; matrix products, arithmetic and copies ran while one was open for 6% of the time, Pallas kernels for 46%

profile of v2, /device:TPU:0, one launch (start us, length us, event | category | flops | bytes accessed | tf_op | source)
XLA Modules:
  0.0 281.8 jit_solution(9021767774387894350)
XLA Ops:
  7.2 0.0 all-gather.2.cloned.1.call-start
  7.2 0.7 all-gather.2.cloned.1.call-update
  7.9 0.0 reduce-scatter.2.cloned.1.call-start
  7.9 1.5 reverse
  9.5 0.1 slice.45
  9.6 0.1 pad.15.clone
  9.6 0.9 slice_reduce_fusion.1
  10.5 0.1 broadcast_in_dim.22
  10.6 0.6 broadcast_in_dim.23.table_ref
  11.2 47.5 %all-gather.2.cloned.1.call-done.whole_ref = bf16[768,4096]{1,0:T(8,128)(2,1)} async-done(((bf16[768,1024]{1,0:T(8,128)(2,1)}), bf16[768,4096]{1,0:T(8,128)(2,1)}) %all-gather.2.cloned.1.call-update) | async-done | bytes 6291472 | tf_op jit(solution)/shard_map/all_gather | solution.py:350
  58.7 0.0 copy-start.6
  58.7 0.0 copy-start.7
  58.7 7.6 %convolution_convert_fusion.1.k_ref = bf16[768,512]{1,0:T(8,128)(2,1)S(1)} fusion(bf16[768,4096]{1,0:T(8,128)(2,1)} %all-gather.2.cloned.1.call-done.whole_ref, bf16[4096,512]{1,0:T(8,128)(2,1)} %param.8), kind=kOutput, calls=%fused_computation.17 | convolution fusion | flops 3221618688 | bytes 11272192 | tf_op jit(solution)/shard_map/dot_general | solution.py:351
  66.2 0.0 copy-start.3
  66.3 0.0 copy-start.8
  66.3 3.6 %collective-permute-start = (bf16[256,512]{1,0:T(8,128)(2,1)S(1)}, bf16[256,512]{1,0:T(8,128)(2,1)S(1)}, u32[]{:S(2)}, u32[]{:S(2)}) collective-permute-start(bf16[256,512]{1,0:T(8,128)(2,1)S(1)} %slice.32), channel_id=1, source_target_pairs={{0,4},{4,8},{8,12},{12,16},{16,20},{20,24},{24,28},{1,5},{5,9},{9,... | collective-permute-start | bytes 786440 | tf_op jit(solution)/shard_map/ppermute | solution.py:23
  69.9 0.0 copy-done.6
  69.9 0.0 copy-done.7
  69.9 3.4 %convolution_convert_fusion.v_ref = bf16[768,512]{1,0:T(8,128)(2,1)S(1)} fusion(bf16[768,4096]{1,0:T(8,128)(2,1)S(1)} %copy-done.6, bf16[4096,512]{1,0:T(8,128)(2,1)S(1)} %copy-done.7), kind=kOutput, calls=%fused_computation.16 | convolution fusion | flops 3221618688 | bytes 11272192 | tf_op jit(solution)/shard_map/dot_general | solution.py:352
  73.3 0.0 copy-done.3
  73.4 0.0 copy-start.4
  73.4 3.4 %collective-permute-start.1 = (bf16[256,512]{1,0:T(8,128)(2,1)S(1)}, bf16[256,512]{1,0:T(8,128)(2,1)S(1)}, u32[]{:S(2)}, u32[]{:S(2)}) collective-permute-start(bf16[256,512]{1,0:T(8,128)(2,1)S(1)} %slice.33), channel_id=1, source_target_pairs={{0,4},{4,8},{8,12},{12,16},{16,20},{20,24},{24,28},{1,5},{5,9},{9,... | collective-permute-start | bytes 786440 | tf_op jit(solution)/shard_map/ppermute | solution.py:23
  76.8 0.0 copy-done.8
  76.8 4.3 %convolution_convert_fusion.2.q_ref = bf16[768,512]{1,0:T(8,128)(2,1)} fusion(bf16[768,4096]{1,0:T(8,128)(2,1)S(1)} %copy-done.6, bf16[4096,512]{1,0:T(8,128)(2,1)S(1)} %copy-done.8), kind=kOutput, calls=%fused_computation.18 | convolution fusion | flops 3221618688 | bytes 11272192 | tf_op jit(solution)/shard_map/dot_general | solution.py:357
  81.1 0.0 copy-done.4
  81.1 0.0 collective-permute-done.pk_ref
  81.1 0.0 copy-start.9
  81.1 1.4 collective-permute-done.1.pv_ref
  82.5 0.0 copy-start.10
  82.5 0.0 copy-done.9
  82.5 0.7 copy-done.10
  83.2 17.2 %shard_map.101 = (bf16[768,512]{1,0:T(8,128)(2,1)}, bf16[512,512]{1,0:T(8,128)(2,1)}, bf16[512,512]{1,0:T(8,128)(2,1)}, f32[256,512]{1,0:T(8,128)}, f32[256,512]...) custom-call(s32[1]{0:T(128)} %bitcast.first_ref, bf16[768,512]{1,0:T(8,128)(2,1)} %convolution_convert_fusion.2.q_ref, ...), custom_call_target="tpu_custom_call" | custom-call | flops 1509949440 | bytes 5505024 | tf_op jit(solution)/shard_map/pallas_call | solution.py:142
  100.3 1.5 collective-permute-start.2
  101.8 14.3 %collective-permute-done.2 = bf16[2,256,512]{2,1,0:T(8,128)(2,1)S(1)} collective-permute-done((bf16[2,256,512]{2,1,0:T(8,128)(2,1)}, bf16[2,256,512]{2,1,0:T(8,128)(2,1)S(1)}, u32[]{:S(2)}, u32[]{:S(2)}) %collective-permute-start.2) | collective-permute-done | bytes 524320 | tf_op jit(solution)/shard_map/ppermute | solution.py:23
  116.1 1.4 fusion.19
  117.5 15.2 %fusion.6 = bf16[768,4096]{1,0:T(8,128)(2,1)} fusion(bf16[4096,512]{1,0:T(8,128)(2,1)} %param.9, bf16[4096,512]{1,0:T(8,128)(2,1)} %param.8, bf16[4096,512]{1,0:T(8,128)(2,1)} %param.7, bf16[256,512]{1,0:T(8,128)(2,1)S(1)} %get-tuple-element.30, bf16[512,512]{1,0:T(8,128)(2,1)} %get-tuple-element.21, bf16[256,512]{1,0:T(8,128)(2,1)S(1)} %get-tuple-element.29, ...), kind=kOutput, calls=%fused_computation.6 | convolution fusion | flops 9716367360 | bytes 21233664 | tf_op jit(solution)/shard_map/dot_general | solution.py:33
  132.8 0.0 copy-start.5
  132.8 0.0 copy-start.1
  132.8 0.0 copy-start.2
  132.8 0.0 reduce-scatter.2.cloned.1.call-update
  132.8 0.7 copy-done.5
  133.5 0.6 copy.14
  134.1 0.0 copy-done.1
  134.1 0.0 copy-done.2
  134.1 1.2 pad_maximum_fusion
  135.3 130.7 %shard_map.102 = (f32[512,512]{1,0:T(8,128)}, f32[512,512]{1,0:T(8,128)}, f32[512,512]{1,0:T(8,128)}, f32[4,512]{1,0:T(4,128)}) custom-call(bf16[768,4096]{1,0:T(8,128)(2,1)} %all-gather.2.cloned.1.call-done.whole_ref, bf16[768,512]{1,0:T(8,128)(2,1)} %get-tuple-element.17.dq_ref, bf16[768,512]{1,0:T(8,128)(2,1)} %get-tuple-element.23.dk_ref, ...), custom_call_target="tpu_custom_call" | custom-call | flops 9663676416 | bytes 400000000 | tf_op jit(solution)/shard_map/pallas_call | solution.py:323
  266.0 0.0 copy-start
  266.0 0.9 slice.29
  266.9 0.8 slice_reduce_fusion
  267.6 0.1 copy.11
  267.7 0.3 reverse.1
  268.0 0.1 slice.46
  268.1 0.7 slice_add_fusion
  268.8 0.7 pad_maximum_fusion.3
  269.4 0.0 reduce-scatter.2.cloned.1.call-done
  269.4 2.3 copy.18
  271.7 2.3 copy.19
  274.0 0.0 copy-done
  274.0 1.0 copy.20
  (4 shorter events, 0.0 us)
Async XLA Ops:
  7.2 51.5 %all-gather.2.cloned.1.call-start = ((), (), s32[]{:S(2)}) async-start(), calls=%async_computation.1 | async-start | bytes 7864320 | tf_op jit(solution)/shard_map/all_gather | solution.py:350
  7.9 261.5 %reduce-scatter.2.cloned.1.call-start = ((), (), s32[]{:S(2)}) async-start(), calls=%async_computation.2 | async-start | bytes 7864320 | tf_op jit(solution)/shard_map/reduce_scatter | solution.py:366
  58.7 11.3 %copy-start.6 = (bf16[768,4096]{1,0:T(8,128)(2,1)S(1)}, bf16[768,4096]{1,0:T(8,128)(2,1)}, u32[]{:S(2)}) copy-start(bf16[768,4096]{1,0:T(8,128)(2,1)} %all-gather.2.cloned.1.call-done.whole_ref) | copy-start | bytes 18874372
  58.7 11.3 %copy-start.7 = (bf16[4096,512]{1,0:T(8,128)(2,1)S(1)}, bf16[4096,512]{1,0:T(8,128)(2,1)}, u32[]{:S(2)}) copy-start(bf16[4096,512]{1,0:T(8,128)(2,1)} %param.9) | copy-start | bytes 12582916
  66.2 7.1 %copy-start.3 = (bf16[768,512]{1,0:T(8,128)(2,1)}, bf16[768,512]{1,0:T(8,128)(2,1)S(1)}, u32[]{:S(2)}) copy-start(bf16[768,512]{1,0:T(8,128)(2,1)S(1)} %convolution_convert_fusion.1.k_ref) | copy-start | bytes 2359300
  66.3 10.5 %copy-start.8 = (bf16[4096,512]{1,0:T(8,128)(2,1)S(1)}, bf16[4096,512]{1,0:T(8,128)(2,1)}, u32[]{:S(2)}) copy-start(bf16[4096,512]{1,0:T(8,128)(2,1)} %param.7) | copy-start | bytes 12582916
  66.3 14.8 %collective-permute-start = (bf16[256,512]{1,0:T(8,128)(2,1)S(1)}, bf16[256,512]{1,0:T(8,128)(2,1)S(1)}, u32[]{:S(2)}, u32[]{:S(2)}) collective-permute-start(bf16[256,512]{1,0:T(8,128)(2,1)S(1)} %slice.32), channel_id=1, source_target_pairs={{0,4},{4,8},{8,12},{12,16},{16,20},{20,24},{24,28},{1,5},{5,9},{9,... | collective-permute-start | bytes 786440 | tf_op jit(solution)/shard_map/ppermute | solution.py:23
  73.4 7.7 %copy-start.4 = (bf16[768,512]{1,0:T(8,128)(2,1)}, bf16[768,512]{1,0:T(8,128)(2,1)S(1)}, u32[]{:S(2)}) copy-start(bf16[768,512]{1,0:T(8,128)(2,1)S(1)} %convolution_convert_fusion.v_ref) | copy-start | bytes 2359300
  73.4 9.1 %collective-permute-start.1 = (bf16[256,512]{1,0:T(8,128)(2,1)S(1)}, bf16[256,512]{1,0:T(8,128)(2,1)S(1)}, u32[]{:S(2)}, u32[]{:S(2)}) collective-permute-start(bf16[256,512]{1,0:T(8,128)(2,1)S(1)} %slice.33), channel_id=1, source_target_pairs={{0,4},{4,8},{8,12},{12,16},{16,20},{20,24},{24,28},{1,5},{5,9},{9,... | collective-permute-start | bytes 786440 | tf_op jit(solution)/shard_map/ppermute | solution.py:23
  81.1 1.4 copy-start.9
  82.5 0.7 copy-start.10
  100.3 15.8 %collective-permute-start.2 = (bf16[2,256,512]{2,1,0:T(8,128)(2,1)}, bf16[2,256,512]{2,1,0:T(8,128)(2,1)S(1)}, u32[]{:S(2)}, u32[]{:S(2)}) collective-permute-start(bf16[2,256,512]{2,1,0:T(8,128)(2,1)} %get-tuple-element.20), channel_id=1, source_target_pairs={{4,0},{8,4},{12,8},{16,12},{20,16},{24,20},{28,24},{5,1},{9,5},{13... | collective-permute-start | bytes 1572872 | tf_op jit(solution)/shard_map/ppermute | solution.py:23
  132.8 0.7 copy-start.5
  132.8 1.3 copy-start.1
  132.8 1.3 copy-start.2
  266.0 8.0 %copy-start = (f32[512,512]{1,0:T(8,128)S(1)}, f32[512,512]{1,0:T(8,128)}, u32[]{:S(2)}) copy-start(f32[512,512]{1,0:T(8,128)} %get-tuple-element.41) | copy-start | bytes 3145732
Sparse Core Ops, SparseCore 0:
  9.5 49.0 all-gather.1
  132.9 58.1 reduce-scatter.1

commit v3 on v2

--- a/solution.py
+++ b/solution.py
@@ -52,8 +52,7 @@
     q_ref,
     k_ref,
     v_ref,
-    pk_ref,
-    pv_ref,
+    prev_ref,
     g_ref,
     table_ref,
     dq_ref,
@@ -69,9 +68,9 @@
     dv_all,
 ):
     length = q_ref.shape[0]
-    k_all[:REACH] = pk_ref[...]
+    k_all[:REACH] = prev_ref[0]
     k_all[REACH:] = k_ref[...]
-    v_all[:REACH] = pv_ref[...]
+    v_all[:REACH] = prev_ref[1]
     v_all[REACH:] = v_ref[...]
     dk_all[...] = jnp.zeros_like(dk_all)
     dv_all[...] = jnp.zeros_like(dv_all)
@@ -114,7 +113,7 @@
     table_grad_ref[0] = diagonal_sums(padded)
 
 
-def attention(query, keys, values, prev_keys, prev_values, out_grad, position_bias):
+def attention(query, keys, values, prev, out_grad, position_bias):
     length, width = query.shape
     heads, entries = position_bias.shape
     head = width // heads
@@ -147,8 +146,7 @@
             rows(length),
             rows(length),
             rows(length),
-            rows(REACH),
-            rows(REACH),
+            pl.BlockSpec((2, REACH, head), lambda h: (0, 0, h)),
             rows(length),
             line,
         ],
@@ -179,7 +177,7 @@
         cost_estimate=pl.CostEstimate(
             flops=10 * elements * head, bytes_accessed=14 * length * width, transcendentals=elements
         ),
-    )(first, query, keys, values, prev_keys, prev_values, out_grad, table)
+    )(first, query, keys, values, prev, out_grad, table)
     return outs
 
 
@@ -345,18 +343,233 @@
     )(whole, query_grad, key_grad, value_grad, lines)
 
 
+def gather_kernel(
+    parts,
+    tokens_ref,
+    wq_ref,
+    wk_ref,
+    wv_ref,
+    whole_ref,
+    q_ref,
+    k_ref,
+    v_ref,
+    prev_ref,
+    held,
+    weights,
+    total,
+    halo,
+    halo_got,
+    side_send,
+    side_recv,
+    far_send,
+    far_recv,
+    relay_send,
+    relay_recv,
+    halo_send,
+    halo_recv,
+    load_sem,
+    store_sem,
+):
+    me = lax.axis_index("tp")
+    seat = lax.axis_index("sp")
+    seats = lax.axis_size("sp")
+    partner = me + 1 - 2 * lax.rem(me, 2)
+    chunks = held.shape[0]
+    block = tokens_ref.shape[1]
+    width = q_ref.shape[1]
+    pairs = parts // 2
+    matrices = (wq_ref, wk_ref, wv_ref)
+
+    def source(device, away):
+        return lax.rem(device + parts - 2 * away, parts)
+
+    order = [me, partner]
+    for away in range(1, pairs):
+        order += [source(me, away), source(partner, away)]
+
+    def load(slot, matrix):
+        start = pl.multiple_of(order[slot] * block, block)
+        return pltpu.make_async_copy(
+            matrices[matrix].at[pl.ds(start, block)],
+            weights.at[slot, matrix],
+            load_sem.at[slot, matrix],
+        )
+
+    for slot in range(parts):
+        for matrix in range(3):
+            load(slot, matrix).start()
+
+    barrier = pltpu.get_barrier_semaphore()
+    for ahead in range(1, parts):
+        pl.semaphore_signal(
+            barrier,
+            inc=1,
+            device_id={"tp": lax.rem(me + ahead, parts)},
+            device_id_type=pl.DeviceIdType.MESH,
+        )
+    onward = lax.rem(seat + 1, seats)
+    for other in (onward, lax.rem(seat + seats - 1, seats)):
+        pl.semaphore_signal(
+            barrier, inc=1, device_id={"sp": other}, device_id_type=pl.DeviceIdType.MESH
+        )
+    pl.semaphore_wait(barrier, parts + 1)
+
+    def rows(chunk):
+        return pl.ds(chunk * REACH, REACH)
+
+    def remote(src, dst, send, recv, device):
+        return pltpu.make_async_remote_copy(
+            src_ref=src,
+            dst_ref=dst,
+            send_sem=send,
+            recv_sem=recv,
+            device_id=device,
+            device_id_type=pl.DeviceIdType.MESH,
+        )
+
+    def far(chunk, away):
+        return remote(
+            tokens_ref.at[rows(chunk)],
+            held.at[chunk, me],
+            far_send.at[chunk, away - 1],
+            far_recv.at[chunk, away - 1],
+            {"tp": lax.rem(me + 2 * away, parts)},
+        )
+
+    def side(chunk):
+        return remote(
+            tokens_ref.at[rows(chunk)],
+            held.at[chunk, me],
+            side_send.at[chunk],
+            side_recv.at[chunk],
+            {"tp": partner},
+        )
+
+    def relay(chunk, away):
+        place = held.at[chunk, source(me, away)]
+        return remote(
+            place,
+            place,
+            relay_send.at[chunk, away - 1],
+            relay_recv.at[chunk, away - 1],
+            {"tp": partner},
+        )
+
+    def neighbour():
+        return remote(halo, halo_got, halo_send, halo_recv, {"sp": onward})
+
+    def store(chunk, slot):
+        start = pl.multiple_of(order[slot] * block, block)
+        src = tokens_ref.at[rows(chunk)] if slot == 0 else held.at[chunk, order[slot]]
+        return pltpu.make_async_copy(
+            src, whole_ref.at[rows(chunk), pl.ds(start, block)], store_sem.at[chunk, slot]
+        )
+
+    def add(chunk, slot, value):
+        for matrix in range(3):
+            term = jnp.dot(value, weights[slot, matrix], preferred_element_type=jnp.float32)
+            if slot == 0:
+                total[matrix, chunk] = term
+            else:
+                total[matrix, chunk] += term
+
+    backwards = list(range(chunks))[::-1]
+    for chunk in backwards:
+        for away in range(1, pairs):
+            far(chunk, away).start()
+        side(chunk).start()
+    for slot in range(2):
+        for matrix in range(3):
+            load(slot, matrix).wait()
+        for chunk in backwards:
+            if slot == 1:
+                side(chunk).wait_recv()
+            store(chunk, slot).start()
+            value = tokens_ref[rows(chunk)] if slot == 0 else held[chunk, partner]
+            add(chunk, slot, value)
+    for slot in range(2, parts):
+        for matrix in range(3):
+            load(slot, matrix).wait()
+    outs = (q_ref, k_ref, v_ref)
+    for chunk in backwards:
+        for away in range(1, pairs):
+            far(chunk, away).wait_recv()
+            relay(chunk, away).start()
+            store(chunk, 2 * away).start()
+            add(chunk, 2 * away, held[chunk, source(me, away)])
+        for away in range(1, pairs):
+            relay(chunk, away).wait_recv()
+            store(chunk, 2 * away + 1).start()
+            add(chunk, 2 * away + 1, held[chunk, source(partner, away)])
+        for matrix in range(3):
+            outs[matrix][rows(chunk)] = total[matrix, chunk].astype(jnp.bfloat16)
+        if chunk == chunks - 1:
+            halo[0] = total[1, chunk].astype(jnp.bfloat16)
+            halo[1] = total[2, chunk].astype(jnp.bfloat16)
+            neighbour().start()
+    neighbour().wait()
+    prev_ref[...] = halo_got[...]
+    for chunk in backwards:
+        side(chunk).wait_send()
+        for away in range(1, pairs):
+            far(chunk, away).wait_send()
+            relay(chunk, away).wait_send()
+        for slot in range(parts):
+            store(chunk, slot).wait()
+
+
+def project(tokens, query_weight, key_weight, value_weight):
+    parts = lax.axis_size("tp")
+    length, block = tokens.shape
+    width = query_weight.shape[1]
+    chunks = length // REACH
+    pairs = parts // 2
+    vmem = pl.BlockSpec(memory_space=pltpu.VMEM)
+    anywhere = pl.BlockSpec(memory_space=pl.ANY)
+    narrow = jax.ShapeDtypeStruct((length, width), jnp.bfloat16)
+    dma = pltpu.SemaphoreType.DMA
+    return pl.pallas_call(
+        functools.partial(gather_kernel, parts),
+        in_specs=[vmem, anywhere, anywhere, anywhere],
+        out_specs=[anywhere, vmem, vmem, vmem, vmem],
+        out_shape=[
+            jax.ShapeDtypeStruct((length, block * parts), jnp.bfloat16),
+            narrow,
+            narrow,
+            narrow,
+            jax.ShapeDtypeStruct((2, REACH, width), jnp.bfloat16),
+        ],
+        scratch_shapes=[
+            pltpu.VMEM((chunks, parts, REACH, block), jnp.bfloat16),
+            pltpu.VMEM((parts, 3, block, width), jnp.bfloat16),
+            pltpu.VMEM((3, chunks, REACH, width), jnp.float32),
+            pltpu.VMEM((2, REACH, width), jnp.bfloat16),
+            pltpu.VMEM((2, REACH, width), jnp.bfloat16),
+            dma((chunks,)),
+            dma((chunks,)),
+            dma((chunks, pairs - 1)),
+            dma((chunks, pairs - 1)),
+            dma((chunks, pairs - 1)),
+            dma((chunks, pairs - 1)),
+            dma(()),
+            dma(()),
+            dma((parts, 3)),
+            dma((chunks, parts)),
+        ],
+        compiler_params=pltpu.CompilerParams(
+            collective_id=1, has_side_effects=True, vmem_limit_bytes=56 * 1024 * 1024
+        ),
+        cost_estimate=pl.CostEstimate(
+            flops=6 * length * block * parts * width, bytes_accessed=150_000_000, transcendentals=0
+        ),
+    )(tokens, query_weight, key_weight, value_weight)
+
+
 def shards(tokens, query_weight, key_weight, value_weight, position_bias, out_grad):
     weights = jnp.concatenate([query_weight, key_weight, value_weight], axis=1)
-    whole = lax.all_gather(tokens, "tp", axis=1, tiled=True)
-    keys = jnp.dot(whole, key_weight, preferred_element_type=jnp.float32).astype(jnp.bfloat16)
-    values = jnp.dot(whole, value_weight, preferred_element_type=jnp.float32).astype(jnp.bfloat16)
-    length = keys.shape[0]
-    prev_keys, prev_values = from_behind(
-        (keys[length - REACH :], values[length - REACH :]), "sp", 1
-    )
-    query = jnp.dot(whole, query_weight, preferred_element_type=jnp.float32).astype(jnp.bfloat16)
+    whole, query, keys, values, prev = project(tokens, query_weight, key_weight, value_weight)
     query_grad, key_body, value_body, key_tail, value_tail, back, lines = attention(
-        query, keys, values, prev_keys, prev_values, out_grad, position_bias
+        query, keys, values, prev, out_grad, position_bias
     )
     after = from_behind(back, "sp", -1)
     key_grad = jnp.concatenate([key_body, (key_tail + after[0]).astype(jnp.bfloat16)])

time: 282 us -> 257 us (0.911)
  waiting for transfers between devices: 63.8 us -> 15.4 us
  Pallas kernels: 148 us -> 195 us
  matrix products: 30.5 us -> 15.2 us
  starting transfers between devices: 8.58 us -> 1.51 us
    all_gather x1 -> x0, waiting for transfers between devices: 47.5 us -> none  [shards(): whole = lax.all_gather(tokens, 'tp', axis=1, tiled=True)]
    pallas_call x0 -> x1, Pallas kernels: none -> 47 us  [project(): pl.pallas_call(functools.partial(gather_kernel, parts), in_specs=[vmem, a...]
    dot_general x3 -> x0, matrix products: 15.2 us -> none  [the longest x1 7.55 us: shards(): jnp.dot(whole, key_weight, preferred_element_type=jnp.float32)]
    ppermute x3 -> x1, starting transfers between devices: 8.51 us -> 1.47 us  [from_behind(): lax.ppermute(value, axis, [(source, source + steps) for source in range(l...]
    unnamed x30 -> x16, local copies, waits for them, and re-layouts: 9.47 us -> 8.72 us
    ppermute x3 -> x1, waiting for transfers between devices: 15.7 us -> 15.3 us  [from_behind(): lax.ppermute(value, axis, [(source, source + steps) for source in range(l...]
  transfers between devices with their start and end apart: 5 -> 2, of which waited for: 3 -> 1; matrix products, arithmetic and copies ran while one was open for 6% -> 2% of each run, Pallas kernels for 46% -> 51%
where the time goes in v3:
time: 257 us
  Pallas kernels  195 us (76%)
  waiting for transfers between devices  15.4 us (6%)
  matrix products  15.2 us (6%)
  between operations  14.1 us (5%)
  local copies, waits for them, and re-layouts  11.3 us (4%)
  other arithmetic  4.7 us (2%)
    pallas_call x1, Pallas kernels, weight_grads(): pl.pallas_call(functools.partial(ring_kernel, count), in_specs=[vmem] * 5...  130 us
    pallas_call x1, Pallas kernels, project(): pl.pallas_call(functools.partial(gather_kernel, parts), in_specs=[vmem, a...  47 us
    pallas_call x1, Pallas kernels, attention(): pl.pallas_call(functools.partial(attention_kernel, factor), grid=(heads,)...  17.1 us
    ppermute x1, waiting for transfers between devices, from_behind(): lax.ppermute(value, axis, [(source, source + steps) for source in range(l...  15.3 us
    dot_general x1, matrix products, contract_cols(): lax.dot_general(left, right, (((1,), (1,)), ((), ())), preferred_element_...  15.2 us
    unnamed x16, local copies, waits for them, and re-layouts  8.72 us
  transfers between devices with their start and end apart: 2, of which 1 were waited for; matrix products, arithmetic and copies ran while one was open for 2% of the time, Pallas kernels for 51%

profile of v3, /device:TPU:0, one launch (start us, length us, event | category | flops | bytes accessed | tf_op | source)
XLA Modules:
  0.0 256.7 jit_solution(14970227267842754484)
XLA Ops:
  7.2 0.0 reduce-scatter.2.cloned.1.call-start
  7.2 0.9 slice_reduce_fusion.1
  8.1 1.5 reverse
  9.6 0.1 slice.35
  9.7 0.1 pad.15.clone
  9.8 0.1 broadcast_in_dim.22
  9.9 0.6 broadcast_in_dim.23.table_ref
  10.5 47.0 %shard_map.101 = (bf16[768,4096]{1,0:T(8,128)(2,1)}, bf16[768,512]{1,0:T(8,128)(2,1)}, bf16[768,512]{1,0:T(8,128)(2,1)}, bf16[768,512]{1,0:T(8,128)(2,1)}, bf16[2,256,512]{2,1,0:T(8,128)(2,1)}) custom-call(bf16[768,1024]{1,0:T(8,128)(2,1)} %tokens_ref.1, bf16[4096,512]{1,0:T(8,128)(2,1)} %wq_ref.1, bf16[4096,512]{1,0:T(8,128)(2,1)} %wk_ref.1, ...), custom_call_target="tpu_custom_call" | custom-call | flops 9663676416 | bytes 150000000 | tf_op jit(solution)/shard_map/pallas_call | solution.py:531
  57.4 17.1 %shard_map.102 = (bf16[768,512]{1,0:T(8,128)(2,1)}, bf16[512,512]{1,0:T(8,128)(2,1)}, bf16[512,512]{1,0:T(8,128)(2,1)}, f32[256,512]{1,0:T(8,128)}, f32[256,512]...) custom-call(s32[1]{0:T(128)} %bitcast.first_ref, bf16[768,512]{1,0:T(8,128)(2,1)} %get-tuple-element.22.q_ref, ...), custom_call_target="tpu_custom_call" | custom-call | flops 1509949440 | bytes 5505024 | tf_op jit(solution)/shard_map/pallas_call | solution.py:141
  74.6 1.5 collective-permute-start
  76.1 15.3 %collective-permute-done = bf16[2,256,512]{2,1,0:T(8,128)(2,1)S(1)} collective-permute-done((bf16[2,256,512]{2,1,0:T(8,128)(2,1)}, bf16[2,256,512]{2,1,0:T(8,128)(2,1)S(1)}, u32[]{:S(2)}, u32[]{:S(2)}) %collective-permute-start) | collective-permute-done | bytes 524320 | tf_op jit(solution)/shard_map/ppermute | solution.py:23
  91.4 1.4 fusion.19
  92.8 15.2 %fusion.6 = bf16[768,4096]{1,0:T(8,128)(2,1)} fusion(bf16[4096,512]{1,0:T(8,128)(2,1)} %wv_ref.1, bf16[4096,512]{1,0:T(8,128)(2,1)} %wk_ref.1, bf16[4096,512]{1,0:T(8,128)(2,1)} %wq_ref.1, bf16[256,512]{1,0:T(8,128)(2,1)S(1)} %get-tuple-element.40, bf16[512,512]{1,0:T(8,128)(2,1)} %get-tuple-element.30, bf16[256,512]{1,0:T(8,128)(2,1)S(1)} %get-tuple-element.39, ...), kind=kOutput, calls=%fused_computation.6 | convolution fusion | flops 9716367360 | bytes 21233664 | tf_op jit(solution)/shard_map/dot_general | solution.py:33
  108.0 0.0 copy-start.3
  108.0 0.0 copy-start.1
  108.0 0.0 copy-start.2
  108.0 0.0 reduce-scatter.2.cloned.1.call-update
  108.0 0.7 copy-done.3
  108.7 0.6 copy.14
  109.3 0.0 copy-done.1
  109.3 0.0 copy-done.2
  109.3 1.2 pad_maximum_fusion
  110.5 130.4 %shard_map.103 = (f32[512,512]{1,0:T(8,128)}, f32[512,512]{1,0:T(8,128)}, f32[512,512]{1,0:T(8,128)}, f32[4,512]{1,0:T(4,128)}) custom-call(bf16[768,4096]{1,0:T(8,128)(2,1)} %get-tuple-element.32.whole_ref, bf16[768,512]{1,0:T(8,128)(2,1)} %get-tuple-element.26.dq_ref, bf16[768,512]{1,0:T(8,128)(2,1)} %get-tuple-element.33.dk_ref, ...), custom_call_target="tpu_custom_call" | custom-call | flops 9663676416 | bytes 400000000 | tf_op jit(solution)/shard_map/pallas_call | solution.py:321
  240.9 0.0 copy-start
  241.0 0.9 slice.21
  241.8 0.7 slice_reduce_fusion
  242.6 0.1 copy.11
  242.7 0.3 reverse.1
  242.9 0.1 slice.36
  243.0 0.7 slice_add_fusion
  243.7 0.7 pad_maximum_fusion.3
  244.3 0.0 reduce-scatter.2.cloned.1.call-done
  244.3 2.3 copy.18
  246.6 2.3 copy.19
  248.9 0.0 copy-done
  248.9 1.0 copy.20
  (2 shorter events, 0.0 us)
Async XLA Ops:
  7.2 237.2 %reduce-scatter.2.cloned.1.call-start = ((), (), s32[]{:S(2)}) async-start(), calls=%async_computation.1 | async-start | bytes 7864320 | tf_op jit(solution)/shard_map/reduce_scatter | solution.py:579
  74.6 16.8 %collective-permute-start = (bf16[2,256,512]{2,1,0:T(8,128)(2,1)}, bf16[2,256,512]{2,1,0:T(8,128)(2,1)S(1)}, u32[]{:S(2)}, u32[]{:S(2)}) collective-permute-start(bf16[2,256,512]{2,1,0:T(8,128)(2,1)} %get-tuple-element.29), channel_id=1, source_target_pairs={{4,0},{8,4},{12,8},{16,12},{20,16},{24,20},{28,24},{5,1},{9,5},{13... | collective-permute-start | bytes 1572872 | tf_op jit(solution)/shard_map/ppermute | solution.py:23
  108.0 0.7 copy-start.3
  108.0 1.3 copy-start.1
  108.0 1.3 copy-start.2
  240.9 7.9 %copy-start = (f32[512,512]{1,0:T(8,128)S(1)}, f32[512,512]{1,0:T(8,128)}, u32[]{:S(2)}) copy-start(f32[512,512]{1,0:T(8,128)} %get-tuple-element.51) | copy-start | bytes 3145732
Sparse Core Ops, SparseCore 0:
  108.1 55.6 reduce-scatter.1

commit v4 on v3

--- a/solution.py
+++ b/solution.py
@@ -572,12 +572,23 @@
         query, keys, values, prev, out_grad, position_bias
     )
     after = from_behind(back, "sp", -1)
-    key_grad = jnp.concatenate([key_body, (key_tail + after[0]).astype(jnp.bfloat16)])
-    value_grad = jnp.concatenate([value_body, (value_tail + after[1]).astype(jnp.bfloat16)])
-    grads = jnp.concatenate([query_grad, key_grad, value_grad], axis=1)
-    input_part = contract_cols(grads, weights).astype(jnp.bfloat16)
-    input_grad = lax.psum_scatter(input_part, "tp", scatter_dimension=1, tiled=True)
-    barrier = lax.optimization_barrier((key_grad, input_part))
+    body = key_body.shape[0]
+    body_grads = jnp.concatenate([query_grad[:body], key_body, value_body], axis=1)
+    body_part = contract_cols(body_grads, weights).astype(jnp.bfloat16)
+    after, body_part = lax.optimization_barrier((after, body_part))
+    key_last = (key_tail + after[0]).astype(jnp.bfloat16)
+    value_last = (value_tail + after[1]).astype(jnp.bfloat16)
+    last_grads = jnp.concatenate([query_grad[body:], key_last, value_last], axis=1)
+    last_part = contract_cols(last_grads, weights).astype(jnp.bfloat16)
+    key_grad = jnp.concatenate([key_body, key_last])
+    value_grad = jnp.concatenate([value_body, value_last])
+    input_grad = jnp.concatenate(
+        [
+            lax.psum_scatter(part, "tp", scatter_dimension=1, tiled=True)
+            for part in (body_part, last_part)
+        ]
+    )
+    barrier = lax.optimization_barrier((key_grad, body_part, last_part))
     query_weight_grad, key_weight_grad, value_weight_grad, lines = weight_grads(
         whole, query_grad, barrier[0], value_grad, lines[:, 0]
     )

time: 257 us -> 265 us (1.031)
  waiting for transfers between devices: 15.4 us -> 0.72 us
  matrix products: 15.2 us -> 26.8 us
  local copies, waits for them, and re-layouts: 11.3 us -> 17.9 us
    ppermute x1, waiting for transfers between devices: 15.3 us -> 0.01 us  [from_behind(): lax.ppermute(value, axis, [(source, source + steps) for source in range(l...]
    dot_general x1 -> x2, matrix products: 15.2 us -> 26.8 us  [contract_cols(): lax.dot_general(left, right, (((1,), (1,)), ((), ())), preferred_element_...]
    unnamed x16 -> x34, local copies, waits for them, and re-layouts: 8.72 us -> 14.7 us
    concatenate x1 -> x2, other arithmetic: 1.24 us -> 3.97 us  [the longest x1 2.73 us: shards(): jnp.concatenate([lax.psum_scatter(part, 'tp', scatter_dimension=1, tiled=...]
  transfers between devices with their start and end apart: 2 -> 3, of which waited for: 1 -> 0; matrix products, arithmetic and copies ran while one was open for 2% -> 8% of each run, Pallas kernels for 51% -> 50%
where the time goes in v4:
time: 265 us; the launch traced here: 264 us
  Pallas kernels  197 us (74%)
  matrix products  26.8 us (10%)
  local copies, waits for them, and re-layouts  17.9 us (7%)
  between operations  14.2 us (5%)
  other arithmetic  6.26 us (2%)
    pallas_call x1, Pallas kernels, weight_grads(): pl.pallas_call(functools.partial(ring_kernel, count), in_specs=[vmem] * 5...  133 us
    pallas_call x1, Pallas kernels, project(): pl.pallas_call(functools.partial(gather_kernel, parts), in_specs=[vmem, a...  46.9 us
    dot_general x2, matrix products, contract_cols(): lax.dot_general(left, right, (((1,), (1,)), ((), ())), preferred_element_...  26.8 us
    pallas_call x1, Pallas kernels, attention(): pl.pallas_call(functools.partial(attention_kernel, factor), grid=(heads,)...  17.1 us
    unnamed x34, local copies, waits for them, and re-layouts  14.7 us
  transfers between devices with their start and end apart: 3, of which 0 were waited for; matrix products, arithmetic and copies ran while one was open for 8% of the time, Pallas kernels for 50%

profile of v4, /device:TPU:0, one launch (start us, length us, event | category | flops | bytes accessed | tf_op | source)
XLA Modules:
  0.0 264.3 jit_solution(12741119992338837707)
XLA Ops:
  7.2 0.0 reduce-scatter.5.cloned.1.call-start
  7.2 0.9 slice_reduce_fusion.1
  8.1 1.5 reverse
  9.6 0.1 slice.37
  9.7 0.1 pad.15.clone
  9.8 0.1 broadcast_in_dim.22
  9.9 0.6 broadcast_in_dim.23.table_ref
  10.5 46.9 %shard_map.101 = (bf16[768,4096]{1,0:T(8,128)(2,1)}, bf16[768,512]{1,0:T(8,128)(2,1)}, bf16[768,512]{1,0:T(8,128)(2,1)}, bf16[768,512]{1,0:T(8,128)(2,1)}, bf16[2,256,512]{2,1,0:T(8,128)(2,1)}) custom-call(bf16[768,1024]{1,0:T(8,128)(2,1)} %tokens_ref.1, bf16[4096,512]{1,0:T(8,128)(2,1)} %wq_ref.1, bf16[4096,512]{1,0:T(8,128)(2,1)} %wk_ref.1, ...), custom_call_target="tpu_custom_call" | custom-call | flops 9663676416 | bytes 150000000 | tf_op jit(solution)/shard_map/pallas_call | solution.py:531
  57.4 17.1 %shard_map.102 = (bf16[768,512]{1,0:T(8,128)(2,1)}, bf16[512,512]{1,0:T(8,128)(2,1)}, bf16[512,512]{1,0:T(8,128)(2,1)}, f32[256,512]{1,0:T(8,128)}, f32[256,512]...) custom-call(s32[1]{0:T(128)} %bitcast.first_ref, bf16[768,512]{1,0:T(8,128)(2,1)} %get-tuple-element.24.q_ref, ...), custom_call_target="tpu_custom_call" | custom-call | flops 1509949440 | bytes 5505024 | tf_op jit(solution)/shard_map/pallas_call | solution.py:141
  74.5 0.0 copy-start
  74.5 1.7 collective-permute-start
  76.3 2.5 constant_dynamic-update-slice_fusion.2
  78.7 0.0 copy-done
  78.7 0.0 copy-start.1
  78.8 0.6 constant_dynamic-update-slice_fusion.1
  79.3 1.6 copy-done.1
  80.9 0.0 copy-start.6
  80.9 0.0 copy-start.7
  80.9 0.0 copy-start.8
  80.9 0.5 constant_dynamic-update-slice_fusion
  81.5 0.0 copy-start.2
  81.5 4.5 %copy-done.2 = bf16[4096,1536]{1,0:T(8,128)(2,1)} copy-done((bf16[4096,1536]{1,0:T(8,128)(2,1)}, bf16[4096,1536]{1,0:T(8,128)(2,1)S(1)}, u32[]{:S(2)}) %copy-start.2) | copy-done | bytes 12582936
  86.0 0.0 copy-done.6
  86.1 0.0 copy-done.7
  86.1 0.0 copy-done.8
  86.1 0.0 copy-start.9
  86.1 0.0 copy-start.10
  86.1 12.9 %convolution_convert_fusion = bf16[512,4096]{1,0:T(8,128)(2,1)} fusion(bf16[4096,1536]{1,0:T(8,128)(2,1)} %copy-done.2, bf16[512,512]{1,0:T(8,128)(2,1)S(1)} %copy-done.8, bf16[512,512]{1,0:T(8,128)(2,1)S(1)} %copy-done.7, bf16[512,512]{1,0:T(8,128)(2,1)S(1)} %slice.25), kind=kOutput, calls=%fused_computation | convolution fusion | flops 6449266688 | bytes 18350080 | tf_op jit(solution)/shard_map/dot_general | solution.py:33
  99.0 0.0 collective-permute-done
  99.0 0.0 copy-done.9
  99.0 0.0 copy-done.10
  99.0 0.2 fusion.11
  99.2 13.9 %convolution_convert_fusion.1 = bf16[256,4096]{1,0:T(8,128)(2,1)} fusion(bf16[4096,1536]{1,0:T(8,128)(2,1)} %copy-done.2, bf16[256,512]{1,0:T(8,128)(2,1)S(1)} %get-tuple-element.44, bf16[256,512]{1,0:T(8,128)(2,1)S(1)} %get-tuple-element.43, bf16[256,512]{1,0:T(8,128)(2,1)S(1)} %slice.26), kind=kOutput, calls=%fused_computation.1 | convolution fusion | flops 3224633344 | bytes 15466496 | tf_op jit(solution)/shard_map/dot_general | solution.py:33
  113.1 0.0 copy-start.11
  113.2 0.0 reduce-scatter.5.cloned.1.call-update
  113.2 0.0 reduce-scatter.3.cloned.1.call-start
  113.2 0.7 reduce-scatter.3.cloned.1.call-update
  113.9 0.0 copy-done.11
  113.9 0.6 copy.14
  114.5 1.2 pad_maximum_fusion.1
  115.8 132.5 %shard_map.103 = (f32[512,512]{1,0:T(8,128)}, f32[512,512]{1,0:T(8,128)}, f32[512,512]{1,0:T(8,128)}, f32[4,512]{1,0:T(4,128)}) custom-call(bf16[768,4096]{1,0:T(8,128)(2,1)} %get-tuple-element.36.whole_ref, bf16[768,512]{1,0:T(8,128)(2,1)} %get-tuple-element.29.dq_ref, bf16[768,512]{1,0:T(8,128)(2,1)} %get-tuple-element.37.dk_ref, ...), custom_call_target="tpu_custom_call" | custom-call | flops 9663676416 | bytes 400000000 | tf_op jit(solution)/shard_map/pallas_call | solution.py:321
  248.3 0.0 copy-start.5
  248.3 0.0 copy-start.4
  248.3 0.9 slice.29
  249.2 0.8 slice_reduce_fusion
  250.0 0.1 copy.11
  250.1 0.3 reverse.1
  250.4 0.1 slice.38
  250.5 0.7 slice_add_fusion
  251.1 0.7 pad_maximum_fusion.4
  251.8 0.0 copy-start.3
  251.8 0.0 reduce-scatter.5.cloned.1.call-done
  251.8 0.0 reduce-scatter.3.cloned.1.call-done
  251.8 2.7 %pad_maximum_fusion = bf16[768,1024]{1,0:T(8,128)(2,1)} fusion(bf16[256,1024]{1,0:T(8,128)(2,1)} %reduce-scatter.5.cloned.1.call-done, bf16[512,1024]{1,0:T(8,128)(2,1)} %reduce-scatter.3.cloned.1.call-done), kind=kLoop, calls=%fused_computation.7 | loop fusion | flops 3145728 | bytes 3145728 | tf_op jit(solution)/shard_map/concatenate | solution.py:585
  254.5 0.0 copy-done.5
  254.6 1.0 copy.20
  255.5 0.0 copy-done.4
  255.5 1.0 copy.21
  256.5 0.0 copy-done.3
  256.5 1.0 copy.22
  (4 shorter events, 0.1 us)
Async XLA Ops:
  7.2 244.6 %reduce-scatter.5.cloned.1.call-start = ((), (), s32[]{:S(2)}) async-start(), calls=%async_computation.3 | async-start | bytes 2621440 | tf_op jit(solution)/shard_map/reduce_scatter | solution.py:587
  74.5 4.2 %copy-start = (bf16[4096,512]{1,0:T(8,128)(2,1)S(1)}, bf16[4096,512]{1,0:T(8,128)(2,1)}, u32[]{:S(2)}) copy-start(bf16[4096,512]{1,0:T(8,128)(2,1)} %wk_ref.1) | copy-start | bytes 12582916
  74.5 24.5 %collective-permute-start = (bf16[2,256,512]{2,1,0:T(8,128)(2,1)}, bf16[2,256,512]{2,1,0:T(8,128)(2,1)S(1)}, u32[]{:S(2)}, u32[]{:S(2)}) collective-permute-start(bf16[2,256,512]{2,1,0:T(8,128)(2,1)} %get-tuple-element.28), channel_id=1, source_target_pairs={{4,0},{8,4},{12,8},{16,12},{20,16},{24,20},{28,24},{5,1},{9,5},{13... | collective-permute-start | bytes 1572872 | tf_op jit(solution)/shard_map/ppermute | solution.py:23
  78.7 2.2 copy-start.1
  80.9 5.1 %copy-start.6 = (bf16[768,512]{1,0:T(8,128)(2,1)S(1)}, bf16[768,512]{1,0:T(8,128)(2,1)}, u32[]{:S(2)}) copy-start(bf16[768,512]{1,0:T(8,128)(2,1)} %get-tuple-element.29.dq_ref) | copy-start | bytes 2359300
  80.9 5.1 %copy-start.7 = (bf16[512,512]{1,0:T(8,128)(2,1)S(1)}, bf16[512,512]{1,0:T(8,128)(2,1)}, u32[]{:S(2)}) copy-start(bf16[512,512]{1,0:T(8,128)(2,1)} %get-tuple-element.30) | copy-start | bytes 1572868
  80.9 5.1 %copy-start.8 = (bf16[512,512]{1,0:T(8,128)(2,1)S(1)}, bf16[512,512]{1,0:T(8,128)(2,1)}, u32[]{:S(2)}) copy-start(bf16[512,512]{1,0:T(8,128)(2,1)} %get-tuple-element.31) | copy-start | bytes 1572868
  81.5 4.5 %copy-start.2 = (bf16[4096,1536]{1,0:T(8,128)(2,1)}, bf16[4096,1536]{1,0:T(8,128)(2,1)S(1)}, u32[]{:S(2)}) copy-start(bf16[4096,1536]{1,0:T(8,128)(2,1)S(1)} %constant_dynamic-update-slice_fusion) | copy-start | bytes 37748740
  86.1 13.0 %copy-start.9 = (f32[256,512]{1,0:T(8,128)S(1)}, f32[256,512]{1,0:T(8,128)}, u32[]{:S(2)}) copy-start(f32[256,512]{1,0:T(8,128)} %get-tuple-element.33) | copy-start | bytes 1572868
  86.1 12.9 %copy-start.10 = (f32[256,512]{1,0:T(8,128)S(1)}, f32[256,512]{1,0:T(8,128)}, u32[]{:S(2)}) copy-start(f32[256,512]{1,0:T(8,128)} %get-tuple-element.35) | copy-start | bytes 1572868
  113.1 0.8 copy-start.11
  113.2 138.6 %reduce-scatter.3.cloned.1.call-start = ((), (), s32[]{:S(2)}) async-start(), calls=%async_computation.2 | async-start | bytes 5242880 | tf_op jit(solution)/shard_map/reduce_scatter | solution.py:587
  248.3 6.2 %copy-start.5 = (f32[512,512]{1,0:T(8,128)S(1)}, f32[512,512]{1,0:T(8,128)}, u32[]{:S(2)}) copy-start(f32[512,512]{1,0:T(8,128)} %get-tuple-element.53) | copy-start | bytes 3145732
  248.3 7.2 %copy-start.4 = (f32[512,512]{1,0:T(8,128)S(1)}, f32[512,512]{1,0:T(8,128)}, u32[]{:S(2)}) copy-start(f32[512,512]{1,0:T(8,128)} %get-tuple-element.54) | copy-start | bytes 3145732
  251.8 4.7 %copy-start.3 = (f32[512,512]{1,0:T(8,128)S(1)}, f32[512,512]{1,0:T(8,128)}, u32[]{:S(2)}) copy-start(f32[512,512]{1,0:T(8,128)} %get-tuple-element.55) | copy-start | bytes 3145732
Sparse Core Ops, SparseCore 0:
  113.3 30.5 reduce-scatter.4
  146.4 44.4 reduce-scatter.2
